TPU v7x, 32 devices: a whole 2x2x4 slice. The times are simulated.
32 devices in a mesh: grp: 1, ep: 32 (over z, y, x, core).
Axes of the slice: x: 2, y: 2, z: 4, core: 2. Of those that a mesh axis runs over, the one named last changes fastest.
Arguments:
- tokens: bfloat16 [768, 2048], P(('grp', 'ep')), may hold values from -24 to 24, as said below
- routes: int32 [768, 2], P(('grp', 'ep')), may hold values from 0 to 3, all different within a row; in each aligned block of 24 rows (0 to 23, 24 to 47, ...) at most 24 rows name the same one
- gates: float32 [768, 2], P(('grp', 'ep')), may hold values from 0.2 to 1
- w_gate: bfloat16 [32, 2048, 704], P('ep'), may hold values from -0.125 to 0.125
- w_up: bfloat16 [32, 2048, 704], P('ep'), may hold values from -0.125 to 0.125
- w_down: bfloat16 [32, 704, 2048], P('ep'), may hold values from -0.078125 to 0.078125
- norm_gain: float32 [2048], P('ep'), may hold values from 0.1 to 1.9
- norm_bias: float32 [2048], P('ep'), may hold values from -3 to 3
Outputs:
- normed: bfloat16 [768, 2048], P('grp', 'ep')
Inputs may be any that keep to these rules, and one draw needn't show every extreme that they name: `routes`: in each aligned block of 24 rows (the rows of one index of ep) no expert is named by more than 24 rows, a bound that some block reaches. `tokens`: feature scales vary across the width.
All inputs are finite; a program needn't handle non-finite values.
Results may differ from a plain program's by a relative error of at most 0.0032.
Values may be sent and summed in bfloat16 or wider, within the bound.
No kernel may reach another device: no remote copies, remote signals or barrier semaphores. Data moves between devices by JAX's collectives and lax.ppermute only.
A program may use at most 192 MiB of HBM per device.

v0:
```python
import functools

import jax
import jax.numpy as jnp
from jax import lax
from jax.experimental import pallas as pl
from jax.experimental.pallas import tpu as pltpu
from jax.sharding import PartitionSpec as P


SPAN = 8


ALPHA = 8.0**0.25
LN_EPS = 1e-05
CUT = 256
LANES = 128
NT = (((1,), (1,)), ((), ()))


def load_kernel(n, *refs):
    sources, targets, sems = refs[:n], refs[n : 2 * n], refs[2 * n]
    copies = [
        pltpu.make_async_copy(a.at[0], b, sems.at[i])
        for i, (a, b) in enumerate(zip(sources, targets, strict=True))
    ]
    for copy in copies:
        copy.start()
    for copy in copies:
        copy.wait()


def load(*weights):
    n = len(weights)
    weights = [pltpu.with_memory_space_constraint(w, pltpu.HBM) for w in weights]
    return pl.pallas_call(
        functools.partial(load_kernel, n),
        in_specs=[pl.BlockSpec(memory_space=pltpu.HBM)] * n,
        out_specs=[pl.BlockSpec(memory_space=pltpu.VMEM)] * n,
        out_shape=[jax.ShapeDtypeStruct(w.shape[1:], w.dtype) for w in weights],
        scratch_shapes=[pltpu.SemaphoreType.DMA((n,))],
        compiler_params=pltpu.CompilerParams(vmem_limit_bytes=24 << 20),
        name="load",
    )(*weights)


def ffn_kernel(n, *refs):
    blocks, (wg, wu, wd, kept, given, hidden) = refs[:n], refs[n:]
    hid, width = wg.shape
    x = jnp.concatenate([b[...] for b in blocks], axis=0)
    for j in range(0, hid, CUT):
        cols = slice(j, min(j + CUT, hid))
        g = lax.dot_general(x, wg[cols, :], NT, preferred_element_type=jnp.float32)
        u = lax.dot_general(x, wu[cols, :], NT, preferred_element_type=jnp.float32)
        hidden[:, cols] = (g / (1.0 + jnp.exp(-g)) * u).astype(jnp.bfloat16)
    split = kept.shape[0]
    h = hidden[...]
    for j in range(0, width, CUT):
        cols = slice(j, min(j + CUT, width))
        y = jnp.dot(h, wd[:, cols], preferred_element_type=jnp.float32)
        kept[:, cols] = y[:split]
        given[:, cols] = y[split:].astype(jnp.bfloat16)


def ffn(own, other, w_gate, w_up, w_down):
    hid, width = w_gate.shape
    n_own, n_other = (sum(b.shape[0] for b in group) for group in (own, other))
    total = n_own + n_other
    blocks = [*own, *other]
    on_chip = pl.BlockSpec(memory_space=pltpu.VMEM)
    return pl.pallas_call(
        functools.partial(ffn_kernel, len(blocks)),
        in_specs=[on_chip] * (len(blocks) + 3),
        out_specs=[on_chip] * 2,
        out_shape=[
            jax.ShapeDtypeStruct((n_own, width), jnp.float32),
            jax.ShapeDtypeStruct((n_other, width), jnp.bfloat16),
        ],
        scratch_shapes=[pltpu.VMEM((total, hid), jnp.bfloat16)],
        cost_estimate=pl.CostEstimate(
            flops=6 * total * width * hid,
            bytes_accessed=6 * width * hid + 8 * total * width,
            transcendentals=total * hid,
        ),
        compiler_params=pltpu.CompilerParams(vmem_limit_bytes=24 << 20),
        name="ffn",
    )(*blocks, w_gate, w_up, w_down)


def shares_kernel(experts, expert, routes, gates, out):
    first = expert[0]
    spot = lax.broadcasted_iota(jnp.int32, out.shape, 1)
    wanted = lax.rem(first + spot, experts)
    total = jnp.zeros(out.shape, jnp.float32)
    for k in range(routes.shape[1]):
        named = (routes[:, k : k + 1] == wanted) & (spot < experts)
        total = total + jnp.where(named, gates[:, k : k + 1], jnp.float32(0.0))
    out[...] = total


def shares(expert, routes, gates, experts):
    on_chip = pl.BlockSpec(memory_space=pltpu.VMEM)
    return pl.pallas_call(
        functools.partial(shares_kernel, experts),
        in_specs=[pl.BlockSpec(memory_space=pltpu.SMEM), on_chip, on_chip],
        out_specs=on_chip,
        out_shape=jax.ShapeDtypeStruct((routes.shape[0], LANES), jnp.float32),
        compiler_params=pltpu.CompilerParams(vmem_limit_bytes=4 << 20),
        name="shares",
    )(expert, routes, gates)


def on_device(tokens, routes, gates, w_gate, w_up, w_down, norm_gain, norm_bias):
    rows, width = tokens.shape
    devices = lax.axis_size("ep")
    me = lax.axis_index("ep")
    experts = devices // SPAN
    columns = width // devices
    peers = list(range(2, SPAN, 2))
    others = range(1, experts)

    def along(x, k):
        return lax.ppermute(
            x, "ep", [(i, (i + k * SPAN) % devices) for i in range(devices)]
        )

    def across(x, m):
        return lax.ppermute(x, "ep", [(i, i ^ m) for i in range(devices)])

    weights = load(w_gate.transpose(0, 2, 1), w_up.transpose(0, 2, 1), w_down)

    def run(own):
        other = [across(x, 1) for x in own]
        kept, given = ffn(own, other, *weights)
        return kept + across(given, 1).astype(jnp.float32)

    line = jnp.concatenate([along(tokens, k) for k in others], axis=0)
    home = [tokens] + [across(tokens, m) for m in peers]
    remote = {m: across(line, m) for m in peers}
    result = run([line])

    span = line.shape[0]
    parts = {}
    for group in (peers[:2], peers[2:]):
        summed = run([remote[m] for m in group]).astype(jnp.bfloat16)
        for i, m in enumerate(group):
            parts[m] = across(summed[i * span : (i + 1) * span], m)
    for m in peers:
        result = result + parts[m].astype(jnp.float32)
    back = [
        along(result[(k - 1) * rows : k * rows].astype(jnp.bfloat16), -k)
        for k in others
    ]

    summed = run([jnp.concatenate(home, axis=0)])
    mine = summed[:rows]
    for i, m in enumerate(peers):
        part = summed[(i + 1) * rows : (i + 2) * rows].astype(jnp.bfloat16)
        mine = mine + across(part, m).astype(jnp.float32)

    weight = shares(me.reshape(1) // SPAN, routes, gates, experts)

    z = ALPHA * tokens.astype(jnp.float32) + weight[:, :1] * mine
    for k in others:
        z = z + weight[:, k : k + 1] * back[k - 1].astype(jnp.float32)
    mean = jnp.mean(z, axis=1, keepdims=True)
    var = jnp.mean(z * z, axis=1, keepdims=True) - mean * mean
    normed = (z - mean) * lax.rsqrt(var + LN_EPS)
    normed = normed.reshape(rows, devices, columns).transpose(1, 0, 2)
    normed = lax.all_to_all(normed, "ep", 0, 0, tiled=True).reshape(devices * rows, columns)
    return (normed * norm_gain[None, :] + norm_bias[None, :]).astype(jnp.bfloat16)


def solution(mesh):
    placed = (
        P(("grp", "ep"), None),
        P(("grp", "ep"), None),
        P(("grp", "ep"), None),
        P("ep", None, None),
        P("ep", None, None),
        P("ep", None, None),
        P("ep"),
        P("ep"),
    )
    return jax.shard_map(
        on_device, mesh=mesh, in_specs=placed, out_specs=P("grp", "ep"), check_vma=False
    )
```

profile of v0, /device:TPU:0, one launch (start us, length us, event | category | flops | bytes accessed | tf_op | source)
XLA Modules:
  0.0 96.7 jit_solution(6722821693734232219)
XLA Ops:
  0.0 3.1 %collective-permute-start.8 = (bf16[24,2048]{1,0:T(8,128)(2,1)}, bf16[24,2048]{1,0:T(8,128)(2,1)S(1)}, u32[]{:S(2)}, u32[]{:S(2)}) collective-permute-start(bf16[24,2048]{1,0:T(8,128)(2,1)} %param.8), channel_id=1, source_target_pairs={{0,8},{1,9},{2,10},{3,11},{4,12},{5,13},{6,14},{7,15},{8,16},{9,17... | collective-permute-start | bytes 294920 | tf_op jit(solution)/shard_map/ppermute | solution.py:123
  3.1 2.6 %collective-permute-start.9 = (bf16[24,2048]{1,0:T(8,128)(2,1)}, bf16[24,2048]{1,0:T(8,128)(2,1)S(1)}, u32[]{:S(2)}, u32[]{:S(2)}) collective-permute-start(bf16[24,2048]{1,0:T(8,128)(2,1)} %param.8), channel_id=1, source_target_pairs={{0,16},{1,17},{2,18},{3,19},{4,20},{5,21},{6,22},{7,23},{8,24},{9,... | collective-permute-start | bytes 294920 | tf_op jit(solution)/shard_map/ppermute | solution.py:123
  5.6 1.3 %collective-permute-start.10 = (bf16[24,2048]{1,0:T(8,128)(2,1)}, bf16[24,2048]{1,0:T(8,128)(2,1)S(1)}, u32[]{:S(2)}, u32[]{:S(2)}) collective-permute-start(bf16[24,2048]{1,0:T(8,128)(2,1)} %param.8), channel_id=1, source_target_pairs={{0,24},{1,25},{2,26},{3,27},{4,28},{5,29},{6,30},{7,31},{8,0},{9,1... | collective-permute-start | bytes 294920 | tf_op jit(solution)/shard_map/ppermute | solution.py:123
  7.0 1.5 %collective-permute-start = (bf16[24,2048]{1,0:T(8,128)(2,1)}, bf16[24,2048]{1,0:T(8,128)(2,1)S(1)}, u32[]{:S(2)}, u32[]{:S(2)}) collective-permute-start(bf16[24,2048]{1,0:T(8,128)(2,1)} %param.8), channel_id=1, source_target_pairs={{0,2},{1,3},{2,0},{3,1},{4,6},{5,7},{6,4},{7,5},{8,10},{9,11},{10,... | collective-permute-start | bytes 294920 | tf_op jit(solution)/shard_map/ppermute | solution.py:128
  8.5 1.5 %collective-permute-start.1 = (bf16[24,2048]{1,0:T(8,128)(2,1)}, bf16[24,2048]{1,0:T(8,128)(2,1)S(1)}, u32[]{:S(2)}, u32[]{:S(2)}) collective-permute-start(bf16[24,2048]{1,0:T(8,128)(2,1)} %param.8), channel_id=1, source_target_pairs={{0,4},{1,5},{2,6},{3,7},{4,0},{5,1},{6,2},{7,3},{8,12},{9,13},{10,... | collective-permute-start | bytes 294920 | tf_op jit(solution)/shard_map/ppermute | solution.py:128
  10.0 0.9 constant_dynamic-update-slice_fusion.3
  10.9 0.9 collective-permute-done
  11.8 2.4 %collective-permute-start.2 = (bf16[24,2048]{1,0:T(8,128)(2,1)}, bf16[24,2048]{1,0:T(8,128)(2,1)S(1)}, u32[]{:S(2)}, u32[]{:S(2)}) collective-permute-start(bf16[24,2048]{1,0:T(8,128)(2,1)} %param.8), channel_id=1, source_target_pairs={{0,6},{1,7},{2,4},{3,5},{4,2},{5,3},{6,0},{7,1},{8,14},{9,15},{10,... | collective-permute-start | bytes 294920 | tf_op jit(solution)/shard_map/ppermute | solution.py:128
  14.3 3.2 %collective-permute-done.2 = bf16[24,2048]{1,0:T(8,128)(2,1)S(1)} collective-permute-done((bf16[24,2048]{1,0:T(8,128)(2,1)}, bf16[24,2048]{1,0:T(8,128)(2,1)S(1)}, u32[]{:S(2)}, u32[]{:S(2)}) %collective-permute-start.2) | collective-permute-done | bytes 98336 | tf_op jit(solution)/shard_map/ppermute | solution.py:128
  17.7 1.6 %collective-permute-start.13 = (bf16[72,2048]{1,0:T(8,128)(2,1)S(1)}, bf16[72,2048]{1,0:T(8,128)(2,1)S(1)}, u32[]{:S(2)}, u32[]{:S(2)}) collective-permute-start(bf16[72,2048]{1,0:T(8,128)(2,1)S(1)} %constant_dynamic-update-slice_fusion.4.refs_0_), channel_id=1, source_target_pairs={{0,2},{1,3},{2,0},{3,1},{4,6},{5,7},{6,4},{7,5},{8,10},{9,11},{10,... | collective-permute-start | bytes 884744 | tf_op jit(solution)/shard_map/ppermute | solution.py:128
  19.3 1.5 %collective-permute-start.14 = (bf16[72,2048]{1,0:T(8,128)(2,1)S(1)}, bf16[72,2048]{1,0:T(8,128)(2,1)S(1)}, u32[]{:S(2)}, u32[]{:S(2)}) collective-permute-start(bf16[72,2048]{1,0:T(8,128)(2,1)S(1)} %constant_dynamic-update-slice_fusion.4.refs_0_), channel_id=1, source_target_pairs={{0,4},{1,5},{2,6},{3,7},{4,0},{5,1},{6,2},{7,3},{8,12},{9,13},{10,... | collective-permute-start | bytes 884744 | tf_op jit(solution)/shard_map/ppermute | solution.py:128
  21.3 6.4 %collective-permute-done.13.refs_0_ = bf16[72,2048]{1,0:T(8,128)(2,1)S(1)} collective-permute-done((bf16[72,2048]{1,0:T(8,128)(2,1)S(1)}, bf16[72,2048]{1,0:T(8,128)(2,1)S(1)}, u32[]{:S(2)}, u32[]{:S(2)}) %collective-permute-start.13) | collective-permute-done | bytes 294944 | tf_op jit(solution)/shard_map/ppermute | solution.py:128
  27.7 7.0 %collective-permute-done.14.refs_1_ = bf16[72,2048]{1,0:T(8,128)(2,1)S(1)} collective-permute-done((bf16[72,2048]{1,0:T(8,128)(2,1)S(1)}, bf16[72,2048]{1,0:T(8,128)(2,1)S(1)}, u32[]{:S(2)}, u32[]{:S(2)}) %collective-permute-start.14) | collective-permute-done | bytes 294944 | tf_op jit(solution)/shard_map/ppermute | solution.py:128
  34.7 0.8 copy.12.routes
  36.2 3.6 %load.1 = (bf16[704,2048]{1,0:T(8,128)(2,1)S(1)}, bf16[704,2048]{1,0:T(8,128)(2,1)S(1)}, bf16[704,2048]{1,0:T(8,128)(2,1)S(1)}) custom-call(bf16[1,704,2048]{2,1,0:T(8,128)(2,1)} %bitcast.12, bf16[1,704,2048]{2,1,0:T(8,128)(2,1)} %bitcast.13, bf16[1,704,2048]{2,1,0:T(8,128)(2,1)} %refs_2_.1), custom_call_target="tpu_custom_call" | custom-call | tf_op jit(solution)/shard_map/load/pallas_call | solution.py:36
  40.5 2.6 %ffn.4 = (f32[96,2048]{1,0:T(8,128)S(1)}, bf16[96,2048]{1,0:T(8,128)(2,1)S(1)}) custom-call(bf16[96,2048]{1,0:T(8,128)(2,1)S(1)} %constant_dynamic-update-slice_fusion.refs_0_, bf16[96,2048]{1,0:T(8,128)(2,1)S(1)} %collective-permute-done.3.refs_1_, bf16[704,2048]{1,0:T(8,128)(2,1)S(1)} %get-tuple-element.16.refs_2_.refs_4_, ...), custom_call_target="tpu_custom_call" | custom-call | flops 1660944384 | bytes 11796480 | tf_op jit(solution)/shard_map/ffn/pallas_call | solution.py:71
  43.1 2.6 %ffn.5 = (f32[72,2048]{1,0:T(8,128)S(1)}, bf16[72,2048]{1,0:T(8,128)(2,1)S(1)}) custom-call(bf16[72,2048]{1,0:T(8,128)(2,1)S(1)} %constant_dynamic-update-slice_fusion.4.refs_0_, bf16[72,2048]{1,0:T(8,128)(2,1)S(1)} %collective-permute-done.11.refs_1_, bf16[704,2048]{1,0:T(8,128)(2,1)S(1)} %get-tuple-element.16.refs_2_.refs_4_, ...), custom_call_target="tpu_custom_call" | custom-call | flops 1245708288 | bytes 11010048 | tf_op jit(solution)/shard_map/ffn/pallas_call | solution.py:71
  46.3 3.0 %ffn.6 = (f32[144,2048]{1,0:T(8,128)S(1)}, bf16[144,2048]{1,0:T(8,128)(2,1)S(1)}) custom-call(bf16[72,2048]{1,0:T(8,128)(2,1)S(1)} %collective-permute-done.13.refs_0_, bf16[72,2048]{1,0:T(8,128)(2,1)S(1)} %collective-permute-done.14.refs_1_, bf16[72,2048]{1,0:T(8,128)(2,1)S(1)} %collective-permute-done.15.refs_2_, ...), custom_call_target="tpu_custom_call" | custom-call | flops 2491416576 | bytes 13369344 | tf_op jit(solution)/shard_map/ffn/pallas_call | solution.py:71
  49.3 2.6 %ffn.7 = (f32[72,2048]{1,0:T(8,128)S(1)}, bf16[72,2048]{1,0:T(8,128)(2,1)S(1)}) custom-call(bf16[72,2048]{1,0:T(8,128)(2,1)S(1)} %collective-permute-done.20.refs_0_, bf16[72,2048]{1,0:T(8,128)(2,1)S(1)} %collective-permute-done.21.refs_1_, bf16[704,2048]{1,0:T(8,128)(2,1)S(1)} %get-tuple-element.16.refs_2_.refs_4_, ...), custom_call_target="tpu_custom_call" | custom-call | flops 1245708288 | bytes 11010048 | tf_op jit(solution)/shard_map/ffn/pallas_call | solution.py:71
  52.6 1.1 %collective-permute-done.22 = bf16[72,2048]{1,0:T(8,128)(2,1)S(1)} collective-permute-done((bf16[72,2048]{1,0:T(8,128)(2,1)S(1)}, bf16[72,2048]{1,0:T(8,128)(2,1)S(1)}, u32[]{:S(2)}, u32[]{:S(2)}) %collective-permute-start.22) | collective-permute-done | bytes 294944 | tf_op jit(solution)/shard_map/ppermute | solution.py:128
  53.7 1.6 %collective-permute-start.23 = (bf16[72,2048]{1,0:T(8,128)(2,1)S(1)}, bf16[72,2048]{1,0:T(8,128)(2,1)S(1)}, u32[]{:S(2)}, u32[]{:S(2)}) collective-permute-start(bf16[72,2048]{1,0:T(8,128)(2,1)S(1)} %add_convert_fusion.2), channel_id=1, source_target_pairs={{0,6},{1,7},{2,4},{3,5},{4,2},{5,3},{6,0},{7,1},{8,14},{9,15},{10,... | collective-permute-start | bytes 884744 | tf_op jit(solution)/shard_map/ppermute | solution.py:128
  55.5 1.6 %collective-permute-start.18 = (bf16[72,2048]{1,0:T(8,128)(2,1)S(1)}, bf16[72,2048]{1,0:T(8,128)(2,1)S(1)}, u32[]{:S(2)}, u32[]{:S(2)}) collective-permute-start(bf16[72,2048]{1,0:T(8,128)(2,1)S(1)} %get-tuple-element.36), channel_id=1, source_target_pairs={{0,2},{1,3},{2,0},{3,1},{4,6},{5,7},{6,4},{7,5},{8,10},{9,11},{10,... | collective-permute-start | bytes 884744 | tf_op jit(solution)/shard_map/ppermute | solution.py:128
  57.7 1.9 %collective-permute-start.6 = (bf16[24,2048]{1,0:T(8,128)(2,1)S(1)}, bf16[24,2048]{1,0:T(8,128)(2,1)S(1)}, u32[]{:S(2)}, u32[]{:S(2)}) collective-permute-start(bf16[24,2048]{1,0:T(8,128)(2,1)S(1)} %get-tuple-element.40), channel_id=1, source_target_pairs={{0,4},{1,5},{2,6},{3,7},{4,0},{5,1},{6,2},{7,3},{8,12},{9,13},{10,... | collective-permute-start | bytes 294920 | tf_op jit(solution)/shard_map/ppermute | solution.py:128
  59.7 4.9 %collective-permute-done.23 = bf16[72,2048]{1,0:T(8,128)(2,1)S(1)} collective-permute-done((bf16[72,2048]{1,0:T(8,128)(2,1)S(1)}, bf16[72,2048]{1,0:T(8,128)(2,1)S(1)}, u32[]{:S(2)}, u32[]{:S(2)}) %collective-permute-start.23) | collective-permute-done | bytes 294944 | tf_op jit(solution)/shard_map/ppermute | solution.py:128
  64.6 1.5 %collective-permute-start.7 = (bf16[24,2048]{1,0:T(8,128)(2,1)S(1)}, bf16[24,2048]{1,0:T(8,128)(2,1)S(1)}, u32[]{:S(2)}, u32[]{:S(2)}) collective-permute-start(bf16[24,2048]{1,0:T(8,128)(2,1)S(1)} %get-tuple-element.39), channel_id=1, source_target_pairs={{0,6},{1,7},{2,4},{3,5},{4,2},{5,3},{6,0},{7,1},{8,14},{9,15},{10,... | collective-permute-start | bytes 294920 | tf_op jit(solution)/shard_map/ppermute | solution.py:128
  66.1 4.9 %collective-permute-done.18 = bf16[72,2048]{1,0:T(8,128)(2,1)S(1)} collective-permute-done((bf16[72,2048]{1,0:T(8,128)(2,1)S(1)}, bf16[72,2048]{1,0:T(8,128)(2,1)S(1)}, u32[]{:S(2)}, u32[]{:S(2)}) %collective-permute-start.18) | collective-permute-done | bytes 294944 | tf_op jit(solution)/shard_map/ppermute | solution.py:128
  71.8 1.7 %collective-permute-start.25 = (bf16[24,2048]{1,0:T(8,128)(2,1)S(1)}, bf16[24,2048]{1,0:T(8,128)(2,1)S(1)}, u32[]{:S(2)}, u32[]{:S(2)}) collective-permute-start(bf16[24,2048]{1,0:T(8,128)(2,1)S(1)} %get-tuple-element.43), channel_id=1, source_target_pairs={{0,16},{1,17},{2,18},{3,19},{4,20},{5,21},{6,22},{7,23},{8,24},{9,... | collective-permute-start | bytes 294920 | tf_op jit(solution)/shard_map/ppermute | solution.py:123
  74.6 1.9 %collective-permute-done.24 = bf16[24,2048]{1,0:T(8,128)(2,1)S(1)} collective-permute-done((bf16[24,2048]{1,0:T(8,128)(2,1)S(1)}, bf16[24,2048]{1,0:T(8,128)(2,1)S(1)}, u32[]{:S(2)}, u32[]{:S(2)}) %collective-permute-start.24) | collective-permute-done | bytes 98336 | tf_op jit(solution)/shard_map/ppermute | solution.py:123
  76.4 5.3 %collective-permute-done.25 = bf16[24,2048]{1,0:T(8,128)(2,1)S(1)} collective-permute-done((bf16[24,2048]{1,0:T(8,128)(2,1)S(1)}, bf16[24,2048]{1,0:T(8,128)(2,1)S(1)}, u32[]{:S(2)}, u32[]{:S(2)}) %collective-permute-start.25) | collective-permute-done | bytes 98336 | tf_op jit(solution)/shard_map/ppermute | solution.py:123
  82.8 11.3 %all_to_all.5 = f32[32,1,1536]{2,1,0:T(1,128)S(1)} all-to-all(f32[32,1,1536]{2,1,0:T(1,128)S(1)} %reshape.40), channel_id=1, replica_groups=mesh['grp'=1,'ep'=32] {'ep'}, dimensions={0} | all-to-all | bytes 393216 | tf_op jit(solution)/shard_map/all_to_all | solution.py:170
  94.6 1.1 %reduce.8 = f32[32,1536]{1,0:T(8,128)S(1)} reduce(f32[32,1,1536]{2,1,0:T(1,128)S(1)} %all_to_all.5, f32[]{:T(128)} %broadcast.43), dimensions={1}, to_apply=%all_to_all.3.reduce_sub_computation | reduce | bytes 393220 | tf_op jit(solution)/shard_map/all_to_all | solution.py:170
  95.9 0.8 copy.15
  (63 shorter events, 7.9 us)
Async XLA Ops:
  0.0 17.6 %collective-permute-start.8 = (bf16[24,2048]{1,0:T(8,128)(2,1)}, bf16[24,2048]{1,0:T(8,128)(2,1)S(1)}, u32[]{:S(2)}, u32[]{:S(2)}) collective-permute-start(bf16[24,2048]{1,0:T(8,128)(2,1)} %param.8), channel_id=1, source_target_pairs={{0,8},{1,9},{2,10},{3,11},{4,12},{5,13},{6,14},{7,15},{8,16},{9,17... | collective-permute-start | bytes 294920 | tf_op jit(solution)/shard_map/ppermute | solution.py:123
  3.1 14.6 %collective-permute-start.9 = (bf16[24,2048]{1,0:T(8,128)(2,1)}, bf16[24,2048]{1,0:T(8,128)(2,1)S(1)}, u32[]{:S(2)}, u32[]{:S(2)}) collective-permute-start(bf16[24,2048]{1,0:T(8,128)(2,1)} %param.8), channel_id=1, source_target_pairs={{0,16},{1,17},{2,18},{3,19},{4,20},{5,21},{6,22},{7,23},{8,24},{9,... | collective-permute-start | bytes 294920 | tf_op jit(solution)/shard_map/ppermute | solution.py:123
  5.6 12.1 %collective-permute-start.10 = (bf16[24,2048]{1,0:T(8,128)(2,1)}, bf16[24,2048]{1,0:T(8,128)(2,1)S(1)}, u32[]{:S(2)}, u32[]{:S(2)}) collective-permute-start(bf16[24,2048]{1,0:T(8,128)(2,1)} %param.8), channel_id=1, source_target_pairs={{0,24},{1,25},{2,26},{3,27},{4,28},{5,29},{6,30},{7,31},{8,0},{9,1... | collective-permute-start | bytes 294920 | tf_op jit(solution)/shard_map/ppermute | solution.py:123
  7.0 4.8 %collective-permute-start = (bf16[24,2048]{1,0:T(8,128)(2,1)}, bf16[24,2048]{1,0:T(8,128)(2,1)S(1)}, u32[]{:S(2)}, u32[]{:S(2)}) collective-permute-start(bf16[24,2048]{1,0:T(8,128)(2,1)} %param.8), channel_id=1, source_target_pairs={{0,2},{1,3},{2,0},{3,1},{4,6},{5,7},{6,4},{7,5},{8,10},{9,11},{10,... | collective-permute-start | bytes 294920 | tf_op jit(solution)/shard_map/ppermute | solution.py:128
  8.5 5.8 %collective-permute-start.1 = (bf16[24,2048]{1,0:T(8,128)(2,1)}, bf16[24,2048]{1,0:T(8,128)(2,1)S(1)}, u32[]{:S(2)}, u32[]{:S(2)}) collective-permute-start(bf16[24,2048]{1,0:T(8,128)(2,1)} %param.8), channel_id=1, source_target_pairs={{0,4},{1,5},{2,6},{3,7},{4,0},{5,1},{6,2},{7,3},{8,12},{9,13},{10,... | collective-permute-start | bytes 294920 | tf_op jit(solution)/shard_map/ppermute | solution.py:128
  11.8 5.7 %collective-permute-start.2 = (bf16[24,2048]{1,0:T(8,128)(2,1)}, bf16[24,2048]{1,0:T(8,128)(2,1)S(1)}, u32[]{:S(2)}, u32[]{:S(2)}) collective-permute-start(bf16[24,2048]{1,0:T(8,128)(2,1)} %param.8), channel_id=1, source_target_pairs={{0,6},{1,7},{2,4},{3,5},{4,2},{5,3},{6,0},{7,1},{8,14},{9,15},{10,... | collective-permute-start | bytes 294920 | tf_op jit(solution)/shard_map/ppermute | solution.py:128
  17.6 22.9 %collective-permute-start.3 = (bf16[96,2048]{1,0:T(8,128)(2,1)S(1)}, bf16[96,2048]{1,0:T(8,128)(2,1)S(1)}, u32[]{:S(2)}, u32[]{:S(2)}) collective-permute-start(bf16[96,2048]{1,0:T(8,128)(2,1)S(1)} %constant_dynamic-update-slice_fusion.refs_0_), channel_id=1, source_target_pairs={{0,1},{1,0},{2,3},{3,2},{4,5},{5,4},{6,7},{7,6},{8,9},{9,8},{10,11... | collective-permute-start | bytes 1179656 | tf_op jit(solution)/shard_map/ppermute | solution.py:128
  17.7 9.9 %collective-permute-start.13 = (bf16[72,2048]{1,0:T(8,128)(2,1)S(1)}, bf16[72,2048]{1,0:T(8,128)(2,1)S(1)}, u32[]{:S(2)}, u32[]{:S(2)}) collective-permute-start(bf16[72,2048]{1,0:T(8,128)(2,1)S(1)} %constant_dynamic-update-slice_fusion.4.refs_0_), channel_id=1, source_target_pairs={{0,2},{1,3},{2,0},{3,1},{4,6},{5,7},{6,4},{7,5},{8,10},{9,11},{10,... | collective-permute-start | bytes 884744 | tf_op jit(solution)/shard_map/ppermute | solution.py:128
  19.3 15.4 %collective-permute-start.14 = (bf16[72,2048]{1,0:T(8,128)(2,1)S(1)}, bf16[72,2048]{1,0:T(8,128)(2,1)S(1)}, u32[]{:S(2)}, u32[]{:S(2)}) collective-permute-start(bf16[72,2048]{1,0:T(8,128)(2,1)S(1)} %constant_dynamic-update-slice_fusion.4.refs_0_), channel_id=1, source_target_pairs={{0,4},{1,5},{2,6},{3,7},{4,0},{5,1},{6,2},{7,3},{8,12},{9,13},{10,... | collective-permute-start | bytes 884744 | tf_op jit(solution)/shard_map/ppermute | solution.py:128
  20.8 19.1 %collective-permute-start.20 = (bf16[72,2048]{1,0:T(8,128)(2,1)S(1)}, bf16[72,2048]{1,0:T(8,128)(2,1)S(1)}, u32[]{:S(2)}, u32[]{:S(2)}) collective-permute-start(bf16[72,2048]{1,0:T(8,128)(2,1)S(1)} %constant_dynamic-update-slice_fusion.4.refs_0_), channel_id=1, source_target_pairs={{0,6},{1,7},{2,4},{3,5},{4,2},{5,3},{6,0},{7,1},{8,14},{9,15},{10,... | collective-permute-start | bytes 884744 | tf_op jit(solution)/shard_map/ppermute | solution.py:128
  21.3 21.9 %collective-permute-start.11 = (bf16[72,2048]{1,0:T(8,128)(2,1)S(1)}, bf16[72,2048]{1,0:T(8,128)(2,1)S(1)}, u32[]{:S(2)}, u32[]{:S(2)}) collective-permute-start(bf16[72,2048]{1,0:T(8,128)(2,1)S(1)} %constant_dynamic-update-slice_fusion.4.refs_0_), channel_id=1, source_target_pairs={{0,1},{1,0},{2,3},{3,2},{4,5},{5,4},{6,7},{7,6},{8,9},{9,8},{10,11... | collective-permute-start | bytes 884744 | tf_op jit(solution)/shard_map/ppermute | solution.py:128
  27.7 18.6 %collective-permute-start.15 = (bf16[72,2048]{1,0:T(8,128)(2,1)S(1)}, bf16[72,2048]{1,0:T(8,128)(2,1)S(1)}, u32[]{:S(2)}, u32[]{:S(2)}) collective-permute-start(bf16[72,2048]{1,0:T(8,128)(2,1)S(1)} %collective-permute-done.13.refs_0_), channel_id=1, source_target_pairs={{0,1},{1,0},{2,3},{3,2},{4,5},{5,4},{6,7},{7,6},{8,9},{9,8},{10,11... | collective-permute-start | bytes 884744 | tf_op jit(solution)/shard_map/ppermute | solution.py:128
  34.7 11.6 %collective-permute-start.16 = (bf16[72,2048]{1,0:T(8,128)(2,1)S(1)}, bf16[72,2048]{1,0:T(8,128)(2,1)S(1)}, u32[]{:S(2)}, u32[]{:S(2)}) collective-permute-start(bf16[72,2048]{1,0:T(8,128)(2,1)S(1)} %collective-permute-done.14.refs_1_), channel_id=1, source_target_pairs={{0,1},{1,0},{2,3},{3,2},{4,5},{5,4},{6,7},{7,6},{8,9},{9,8},{10,11... | collective-permute-start | bytes 884744 | tf_op jit(solution)/shard_map/ppermute | solution.py:128
  39.9 9.5 %collective-permute-start.21 = (bf16[72,2048]{1,0:T(8,128)(2,1)S(1)}, bf16[72,2048]{1,0:T(8,128)(2,1)S(1)}, u32[]{:S(2)}, u32[]{:S(2)}) collective-permute-start(bf16[72,2048]{1,0:T(8,128)(2,1)S(1)} %collective-permute-done.20.refs_0_), channel_id=1, source_target_pairs={{0,1},{1,0},{2,3},{3,2},{4,5},{5,4},{6,7},{7,6},{8,9},{9,8},{10,11... | collective-permute-start | bytes 884744 | tf_op jit(solution)/shard_map/ppermute | solution.py:128
  43.0 9.4 %collective-permute-start.4 = (bf16[96,2048]{1,0:T(8,128)(2,1)S(1)}, bf16[96,2048]{1,0:T(8,128)(2,1)S(1)}, u32[]{:S(2)}, u32[]{:S(2)}) collective-permute-start(bf16[96,2048]{1,0:T(8,128)(2,1)S(1)} %get-tuple-element.20), channel_id=1, source_target_pairs={{0,1},{1,0},{2,3},{3,2},{4,5},{5,4},{6,7},{7,6},{8,9},{9,8},{10,11... | collective-permute-start | bytes 1179656 | tf_op jit(solution)/shard_map/ppermute | solution.py:128
  45.7 12.0 %collective-permute-start.12 = (bf16[72,2048]{1,0:T(8,128)(2,1)S(1)}, bf16[72,2048]{1,0:T(8,128)(2,1)S(1)}, u32[]{:S(2)}, u32[]{:S(2)}) collective-permute-start(bf16[72,2048]{1,0:T(8,128)(2,1)S(1)} %get-tuple-element.22), channel_id=1, source_target_pairs={{0,1},{1,0},{2,3},{3,2},{4,5},{5,4},{6,7},{7,6},{8,9},{9,8},{10,11... | collective-permute-start | bytes 884744 | tf_op jit(solution)/shard_map/ppermute | solution.py:128
  49.2 6.1 %collective-permute-start.17 = (bf16[144,2048]{1,0:T(8,128)(2,1)S(1)}, bf16[144,2048]{1,0:T(8,128)(2,1)S(1)}, u32[]{:S(2)}, u32[]{:S(2)}) collective-permute-start(bf16[144,2048]{1,0:T(8,128)(2,1)S(1)} %get-tuple-element.24), channel_id=1, source_target_pairs={{0,1},{1,0},{2,3},{3,2},{4,5},{5,4},{6,7},{7,6},{8,9},{9,8},{10,11... | collective-permute-start | bytes 1769480 | tf_op jit(solution)/shard_map/ppermute | solution.py:128
  51.9 1.7 %collective-permute-start.22 = (bf16[72,2048]{1,0:T(8,128)(2,1)S(1)}, bf16[72,2048]{1,0:T(8,128)(2,1)S(1)}, u32[]{:S(2)}, u32[]{:S(2)}) collective-permute-start(bf16[72,2048]{1,0:T(8,128)(2,1)S(1)} %get-tuple-element.26), channel_id=1, source_target_pairs={{0,1},{1,0},{2,3},{3,2},{4,5},{5,4},{6,7},{7,6},{8,9},{9,8},{10,11... | collective-permute-start | bytes 884744 | tf_op jit(solution)/shard_map/ppermute | solution.py:128
  53.7 10.9 %collective-permute-start.23 = (bf16[72,2048]{1,0:T(8,128)(2,1)S(1)}, bf16[72,2048]{1,0:T(8,128)(2,1)S(1)}, u32[]{:S(2)}, u32[]{:S(2)}) collective-permute-start(bf16[72,2048]{1,0:T(8,128)(2,1)S(1)} %add_convert_fusion.2), channel_id=1, source_target_pairs={{0,6},{1,7},{2,4},{3,5},{4,2},{5,3},{6,0},{7,1},{8,14},{9,15},{10,... | collective-permute-start | bytes 884744 | tf_op jit(solution)/shard_map/ppermute | solution.py:128
  55.3 26.5 %copy-start = (bf16[24,2048]{1,0:T(8,128)(2,1)S(1)}, bf16[24,2048]{1,0:T(8,128)(2,1)}, u32[]{:S(2)}) copy-start(bf16[24,2048]{1,0:T(8,128)(2,1)} %param.8) | copy-start | bytes 294916
  55.5 15.5 %collective-permute-start.18 = (bf16[72,2048]{1,0:T(8,128)(2,1)S(1)}, bf16[72,2048]{1,0:T(8,128)(2,1)S(1)}, u32[]{:S(2)}, u32[]{:S(2)}) collective-permute-start(bf16[72,2048]{1,0:T(8,128)(2,1)S(1)} %get-tuple-element.36), channel_id=1, source_target_pairs={{0,2},{1,3},{2,0},{3,1},{4,6},{5,7},{6,4},{7,5},{8,10},{9,11},{10,... | collective-permute-start | bytes 884744 | tf_op jit(solution)/shard_map/ppermute | solution.py:128
  57.1 14.0 %collective-permute-start.19 = (bf16[72,2048]{1,0:T(8,128)(2,1)S(1)}, bf16[72,2048]{1,0:T(8,128)(2,1)S(1)}, u32[]{:S(2)}, u32[]{:S(2)}) collective-permute-start(bf16[72,2048]{1,0:T(8,128)(2,1)S(1)} %get-tuple-element.37), channel_id=1, source_target_pairs={{0,4},{1,5},{2,6},{3,7},{4,0},{5,1},{6,2},{7,3},{8,12},{9,13},{10,... | collective-permute-start | bytes 884744 | tf_op jit(solution)/shard_map/ppermute | solution.py:128
  57.6 15.9 %collective-permute-start.5 = (bf16[24,2048]{1,0:T(8,128)(2,1)S(1)}, bf16[24,2048]{1,0:T(8,128)(2,1)S(1)}, u32[]{:S(2)}, u32[]{:S(2)}) collective-permute-start(bf16[24,2048]{1,0:T(8,128)(2,1)S(1)} %get-tuple-element.38), channel_id=1, source_target_pairs={{0,2},{1,3},{2,0},{3,1},{4,6},{5,7},{6,4},{7,5},{8,10},{9,11},{10,... | collective-permute-start | bytes 294920 | tf_op jit(solution)/shard_map/ppermute | solution.py:128
  57.7 16.3 %collective-permute-start.6 = (bf16[24,2048]{1,0:T(8,128)(2,1)S(1)}, bf16[24,2048]{1,0:T(8,128)(2,1)S(1)}, u32[]{:S(2)}, u32[]{:S(2)}) collective-permute-start(bf16[24,2048]{1,0:T(8,128)(2,1)S(1)} %get-tuple-element.40), channel_id=1, source_target_pairs={{0,4},{1,5},{2,6},{3,7},{4,0},{5,1},{6,2},{7,3},{8,12},{9,13},{10,... | collective-permute-start | bytes 294920 | tf_op jit(solution)/shard_map/ppermute | solution.py:128
  64.6 9.9 %collective-permute-start.7 = (bf16[24,2048]{1,0:T(8,128)(2,1)S(1)}, bf16[24,2048]{1,0:T(8,128)(2,1)S(1)}, u32[]{:S(2)}, u32[]{:S(2)}) collective-permute-start(bf16[24,2048]{1,0:T(8,128)(2,1)S(1)} %get-tuple-element.39), channel_id=1, source_target_pairs={{0,6},{1,7},{2,4},{3,5},{4,2},{5,3},{6,0},{7,1},{8,14},{9,15},{10,... | collective-permute-start | bytes 294920 | tf_op jit(solution)/shard_map/ppermute | solution.py:128
  71.2 24.7 %copy-start.1 = (f32[64]{0:T(128)S(1)}, f32[64]{0:T(128)}, u32[]{:S(2)}) copy-start(f32[64]{0:T(128)} %param.15) | copy-start | bytes 772
  71.2 24.7 %copy-start.2 = (f32[64]{0:T(128)S(1)}, f32[64]{0:T(128)}, u32[]{:S(2)}) copy-start(f32[64]{0:T(128)} %param.14) | copy-start | bytes 772
  71.3 5.2 %collective-permute-start.24 = (bf16[24,2048]{1,0:T(8,128)(2,1)S(1)}, bf16[24,2048]{1,0:T(8,128)(2,1)S(1)}, u32[]{:S(2)}, u32[]{:S(2)}) collective-permute-start(bf16[24,2048]{1,0:T(8,128)(2,1)S(1)} %get-tuple-element.41), channel_id=1, source_target_pairs={{0,24},{1,25},{2,26},{3,27},{4,28},{5,29},{6,30},{7,31},{8,0},{9,1... | collective-permute-start | bytes 294920 | tf_op jit(solution)/shard_map/ppermute | solution.py:123
  71.8 10.0 %collective-permute-start.25 = (bf16[24,2048]{1,0:T(8,128)(2,1)S(1)}, bf16[24,2048]{1,0:T(8,128)(2,1)S(1)}, u32[]{:S(2)}, u32[]{:S(2)}) collective-permute-start(bf16[24,2048]{1,0:T(8,128)(2,1)S(1)} %get-tuple-element.43), channel_id=1, source_target_pairs={{0,16},{1,17},{2,18},{3,19},{4,20},{5,21},{6,22},{7,23},{8,24},{9,... | collective-permute-start | bytes 294920 | tf_op jit(solution)/shard_map/ppermute | solution.py:123
  73.4 8.3 %collective-permute-start.26 = (bf16[24,2048]{1,0:T(8,128)(2,1)S(1)}, bf16[24,2048]{1,0:T(8,128)(2,1)S(1)}, u32[]{:S(2)}, u32[]{:S(2)}) collective-permute-start(bf16[24,2048]{1,0:T(8,128)(2,1)S(1)} %get-tuple-element.42), channel_id=1, source_target_pairs={{0,8},{1,9},{2,10},{3,11},{4,12},{5,13},{6,14},{7,15},{8,16},{9,17... | collective-permute-start | bytes 294920 | tf_op jit(solution)/shard_map/ppermute | solution.py:123
where the time goes:
time: 96.9 us; the launch traced here: 96.7 us
  waiting for transfers between devices  36.3 us (37%)
  starting transfers between devices  27.7 us (29%)
  Pallas kernels  14.3 us (15%)
  blocking collectives  11.3 us (12%)
  local copies, waits for them, and re-layouts  4.84 us (5%)
  other arithmetic  2 us (2%)
    ppermute x21, waiting for transfers between devices, across(): return lax.ppermute(x, 'ep', [(i, i ^ m) for i in range(devices)])  29.1 us
    ppermute x21, starting transfers between devices, across(): return lax.ppermute(x, 'ep', [(i, i ^ m) for i in range(devices)])  18.2 us
    all_to_all x1, blocking collectives, on_device(): lax.all_to_all(normed, 'ep', 0, 0, tiled=True)  11.3 us
    pallas_call x4, Pallas kernels, ffn(): pl.pallas_call(functools.partial(ffn_kernel, len(blocks)), in_specs=[on_c...  10.7 us
    ppermute x6, starting transfers between devices, along(): lax.ppermute(x, 'ep', [(i, (i + k * SPAN) % devices) for i in range(devic...  9.51 us
    ppermute x6, waiting for transfers between devices, along(): lax.ppermute(x, 'ep', [(i, (i + k * SPAN) % devices) for i in range(devic...  7.21 us
    pallas_call x1, Pallas kernels, load(): pl.pallas_call(functools.partial(load_kernel, n), in_specs=[pl.BlockSpec(...  3.56 us
    unnamed x15, local copies, waits for them, and re-layouts  2.85 us
  transfers between devices with their start and end apart: 27, of which 10 were waited for; matrix products, arithmetic and copies ran while one was open for 3% of the time, Pallas kernels for 15%

commit v1 on v0

--- a/solution.py
+++ b/solution.py
@@ -14,7 +14,6 @@
 ALPHA = 8.0**0.25
 LN_EPS = 1e-05
 CUT = 256
-LANES = 128
 NT = (((1,), (1,)), ((), ()))
 
 
@@ -39,7 +38,7 @@
         out_specs=[pl.BlockSpec(memory_space=pltpu.VMEM)] * n,
         out_shape=[jax.ShapeDtypeStruct(w.shape[1:], w.dtype) for w in weights],
         scratch_shapes=[pltpu.SemaphoreType.DMA((n,))],
-        compiler_params=pltpu.CompilerParams(vmem_limit_bytes=24 << 20),
+        compiler_params=pltpu.CompilerParams(vmem_limit_bytes=2 << 20),
         name="load",
     )(*weights)
 
@@ -82,38 +81,55 @@
             bytes_accessed=6 * width * hid + 8 * total * width,
             transcendentals=total * hid,
         ),
-        compiler_params=pltpu.CompilerParams(vmem_limit_bytes=24 << 20),
+        compiler_params=pltpu.CompilerParams(vmem_limit_bytes=10 << 20),
         name="ffn",
     )(*blocks, w_gate, w_up, w_down)
 
 
-def shares_kernel(experts, expert, routes, gates, out):
-    first = expert[0]
-    spot = lax.broadcasted_iota(jnp.int32, out.shape, 1)
-    wanted = lax.rem(first + spot, experts)
-    total = jnp.zeros(out.shape, jnp.float32)
-    for k in range(routes.shape[1]):
-        named = (routes[:, k : k + 1] == wanted) & (spot < experts)
-        total = total + jnp.where(named, gates[:, k : k + 1], jnp.float32(0.0))
-    out[...] = total
-
-
-def shares(expert, routes, gates, experts):
+def shares_kernel(experts, routes, gates, out):
+    first = lax.div(lax.axis_index("ep"), SPAN)
+    for k in range(experts):
+        named = routes[...] == lax.rem(first + k, experts)
+        share = jnp.where(named, gates[...], jnp.float32(0.0))
+        out[k : k + 1, :] = jnp.sum(share, axis=0, keepdims=True)
+
+
+def shares(routes, gates, experts):
     on_chip = pl.BlockSpec(memory_space=pltpu.VMEM)
     return pl.pallas_call(
         functools.partial(shares_kernel, experts),
-        in_specs=[pl.BlockSpec(memory_space=pltpu.SMEM), on_chip, on_chip],
+        in_specs=[on_chip, on_chip],
         out_specs=on_chip,
-        out_shape=jax.ShapeDtypeStruct((routes.shape[0], LANES), jnp.float32),
+        out_shape=jax.ShapeDtypeStruct((experts, routes.shape[1]), jnp.float32),
+        compiler_params=pltpu.CompilerParams(vmem_limit_bytes=2 << 20),
+        name="shares",
+    )(routes, gates)
+
+
+def close_kernel(ks, rows, base, one, two, arrived, *outs):
+    for i, (k, out) in enumerate(zip(ks, outs, strict=True)):
+        total = base[k * rows : (k + 1) * rows, :]
+        for part, at in ((one, k - 1), (two, k - 1), (arrived, i)):
+            total = total + part[at * rows : (at + 1) * rows, :].astype(jnp.float32)
+        out[...] = total.astype(jnp.bfloat16)
+
+
+def close(ks, rows, base, parts, arrived):
+    on_chip = pl.BlockSpec(memory_space=pltpu.VMEM)
+    out = jax.ShapeDtypeStruct((rows, base.shape[1]), jnp.bfloat16)
+    return pl.pallas_call(
+        functools.partial(close_kernel, tuple(ks), rows),
+        in_specs=[on_chip] * 4,
+        out_specs=[on_chip] * len(ks),
+        out_shape=[out] * len(ks),
         compiler_params=pltpu.CompilerParams(vmem_limit_bytes=4 << 20),
-        name="shares",
-    )(expert, routes, gates)
+        name="close",
+    )(base, *parts, arrived)
 
 
 def on_device(tokens, routes, gates, w_gate, w_up, w_down, norm_gain, norm_bias):
     rows, width = tokens.shape
     devices = lax.axis_size("ep")
-    me = lax.axis_index("ep")
     experts = devices // SPAN
     columns = width // devices
     peers = list(range(2, SPAN, 2))
@@ -127,42 +143,55 @@
     def across(x, m):
         return lax.ppermute(x, "ep", [(i, i ^ m) for i in range(devices)])
 
-    weights = load(w_gate.transpose(0, 2, 1), w_up.transpose(0, 2, 1), w_down)
+    projections = load(w_gate.transpose(0, 2, 1), w_up.transpose(0, 2, 1))
+    weights = (*projections, *load(w_down))
 
     def run(own):
         other = [across(x, 1) for x in own]
         kept, given = ffn(own, other, *weights)
         return kept + across(given, 1).astype(jnp.float32)
 
-    line = jnp.concatenate([along(tokens, k) for k in others], axis=0)
-    home = [tokens] + [across(tokens, m) for m in peers]
-    remote = {m: across(line, m) for m in peers}
-    result = run([line])
-
-    span = line.shape[0]
-    parts = {}
-    for group in (peers[:2], peers[2:]):
-        summed = run([remote[m] for m in group]).astype(jnp.bfloat16)
-        for i, m in enumerate(group):
-            parts[m] = across(summed[i * span : (i + 1) * span], m)
+    blocks = [tokens] + [along(tokens, k) for k in others]
+    half = experts // 2
+    first, second, far = peers
+    early = jnp.concatenate(blocks[:half], axis=0)
+    late = jnp.concatenate(blocks[half:], axis=0)
+    remote = {m: (across(early, m), across(late, m)) for m in (first, second)}
+    result = run([early, late])
+
+    upper = across(remote[first][0], second)
+    lower = across(remote[second][1], first)
+
+    ahead = range(half, half + experts // 4)
+    behind = [k for k in others if k not in ahead]
+
+    def pick(x, ks):
+        return jnp.concatenate([x[k * rows : (k + 1) * rows] for k in ks], axis=0)
+
+    summed = {
+        m: run(halves).astype(jnp.bfloat16)
+        for m, halves in (
+            (first, remote[first]), (second, remote[second]), (far, (upper, lower))
+        )
+    }
+    put = {m: across(summed[m][rows:], m) for m in (first, second)}
+    put_lead = across(pick(summed[far], ahead), far)
+    put_tail = across(pick(summed[far], behind), far)
+
+    back = {}
+    for ks, arrived in ((ahead, put_lead), (behind, put_tail)):
+        sums = close(ks, rows, result, [put[first], put[second]], arrived)
+        for k, total in zip(ks, sums, strict=True):
+            back[k] = along(total, -k)
+    mine = result[:rows]
     for m in peers:
-        result = result + parts[m].astype(jnp.float32)
-    back = [
-        along(result[(k - 1) * rows : k * rows].astype(jnp.bfloat16), -k)
-        for k in others
-    ]
-
-    summed = run([jnp.concatenate(home, axis=0)])
-    mine = summed[:rows]
-    for i, m in enumerate(peers):
-        part = summed[(i + 1) * rows : (i + 2) * rows].astype(jnp.bfloat16)
-        mine = mine + across(part, m).astype(jnp.float32)
-
-    weight = shares(me.reshape(1) // SPAN, routes, gates, experts)
-
-    z = ALPHA * tokens.astype(jnp.float32) + weight[:, :1] * mine
+        mine = mine + across(summed[m][:rows], m).astype(jnp.float32)
+
+    weight = shares(routes.T, gates.T, experts)
+
+    z = ALPHA * tokens.astype(jnp.float32) + weight[0][:, None] * mine
     for k in others:
-        z = z + weight[:, k : k + 1] * back[k - 1].astype(jnp.float32)
+        z = z + weight[k][:, None] * back[k].astype(jnp.float32)
     mean = jnp.mean(z, axis=1, keepdims=True)
     var = jnp.mean(z * z, axis=1, keepdims=True) - mean * mean
     normed = (z - mean) * lax.rsqrt(var + LN_EPS)

time: 96.9 us -> 87.1 us (0.90)
  waiting for transfers between devices: 36.3 us -> 24.8 us
  starting transfers between devices: 27.7 us -> 31.1 us
  local copies, waits for them, and re-layouts: 4.84 us -> 3.11 us
    ppermute x21 -> x25, waiting for transfers between devices: 29.1 us -> 15.6 us  [across(): return lax.ppermute(x, 'ep', [(i, i ^ m) for i in range(devices)])]
    ppermute x6, starting transfers between devices: 9.51 us -> 12.8 us  [along(): lax.ppermute(x, 'ep', [(i, (i + k * SPAN) % devices) for i in range(devic...]
    ppermute x6, waiting for transfers between devices: 7.21 us -> 9.21 us  [along(): lax.ppermute(x, 'ep', [(i, (i + k * SPAN) % devices) for i in range(devic...]
    unnamed x15 -> x14, local copies, waits for them, and re-layouts: 2.85 us -> 1.32 us
    pallas_call x1 -> x2, Pallas kernels: 3.56 us -> 4.54 us  [load(): pl.pallas_call(functools.partial(load_kernel, n), in_specs=[pl.BlockSpec(...]
    ppermute x21 -> x25, starting transfers between devices: 18.2 us -> 18.3 us  [across(): return lax.ppermute(x, 'ep', [(i, i ^ m) for i in range(devices)])]
  transfers between devices with their start and end apart: 27 -> 31, of which waited for: 10 -> 9; matrix products, arithmetic and copies ran while one was open for 3% -> 2% of each run, Pallas kernels for 15% -> 17%
where the time goes in v1:
time: 87.1 us; the launch traced here: 86.8 us
  starting transfers between devices  31.1 us (36%)
  waiting for transfers between devices  24.8 us (28%)
  Pallas kernels  15 us (17%)
  blocking collectives  10.7 us (12%)
  local copies, waits for them, and re-layouts  3.11 us (4%)
  other arithmetic  1.84 us (2%)
    ppermute x25, starting transfers between devices, across(): return lax.ppermute(x, 'ep', [(i, i ^ m) for i in range(devices)])  18.3 us
    ppermute x25, waiting for transfers between devices, across(): return lax.ppermute(x, 'ep', [(i, i ^ m) for i in range(devices)])  15.6 us
    ppermute x6, starting transfers between devices, along(): lax.ppermute(x, 'ep', [(i, (i + k * SPAN) % devices) for i in range(devic...  12.8 us
    all_to_all x1, blocking collectives, on_device(): lax.all_to_all(normed, 'ep', 0, 0, tiled=True)  10.7 us
    pallas_call x4, Pallas kernels, ffn(): pl.pallas_call(functools.partial(ffn_kernel, len(blocks)), in_specs=[on_c...  10.3 us
    ppermute x6, waiting for transfers between devices, along(): lax.ppermute(x, 'ep', [(i, (i + k * SPAN) % devices) for i in range(devic...  9.21 us
    pallas_call x2, Pallas kernels, load(): pl.pallas_call(functools.partial(load_kernel, n), in_specs=[pl.BlockSpec(...  4.54 us
  transfers between devices with their start and end apart: 31, of which 9 were waited for; matrix products, arithmetic and copies ran while one was open for 2% of the time, Pallas kernels for 17%

profile of v1, /device:TPU:0, one launch (start us, length us, event | category | flops | bytes accessed | tf_op | source)
XLA Modules:
  0.0 86.8 jit_solution(10649481254429046664)
XLA Ops:
  0.0 4.1 %collective-permute-start.1 = (bf16[24,2048]{1,0:T(8,128)(2,1)}, bf16[24,2048]{1,0:T(8,128)(2,1)S(1)}, u32[]{:S(2)}, u32[]{:S(2)}) collective-permute-start(bf16[24,2048]{1,0:T(8,128)(2,1)} %param.8), channel_id=1, source_target_pairs={{0,16},{1,17},{2,18},{3,19},{4,20},{5,21},{6,22},{7,23},{8,24},{9,... | collective-permute-start | bytes 294920 | tf_op jit(solution)/shard_map/ppermute | solution.py:139
  4.1 1.3 %collective-permute-start.2 = (bf16[24,2048]{1,0:T(8,128)(2,1)}, bf16[24,2048]{1,0:T(8,128)(2,1)S(1)}, u32[]{:S(2)}, u32[]{:S(2)}) collective-permute-start(bf16[24,2048]{1,0:T(8,128)(2,1)} %param.8), channel_id=1, source_target_pairs={{0,24},{1,25},{2,26},{3,27},{4,28},{5,29},{6,30},{7,31},{8,0},{9,1... | collective-permute-start | bytes 294920 | tf_op jit(solution)/shard_map/ppermute | solution.py:139
  5.4 0.7 collective-permute-start
  6.1 0.9 %constant_dynamic-update-slice_fusion.1 = bf16[48,2048]{1,0:T(8,128)(2,1)S(1)} fusion(bf16[24,2048]{1,0:T(8,128)(2,1)} %param.8), kind=kLoop, calls=%fused_computation.20 | loop fusion | bytes 196608
  7.0 3.7 %collective-permute-done.1 = bf16[24,2048]{1,0:T(8,128)(2,1)S(1)} collective-permute-done((bf16[24,2048]{1,0:T(8,128)(2,1)}, bf16[24,2048]{1,0:T(8,128)(2,1)S(1)}, u32[]{:S(2)}, u32[]{:S(2)}) %collective-permute-start.1) | collective-permute-done | bytes 98336 | tf_op jit(solution)/shard_map/ppermute | solution.py:139
  10.7 1.8 %collective-permute-start.13 = (bf16[48,2048]{1,0:T(8,128)(2,1)S(1)}, bf16[48,2048]{1,0:T(8,128)(2,1)S(1)}, u32[]{:S(2)}, u32[]{:S(2)}) collective-permute-start(bf16[48,2048]{1,0:T(8,128)(2,1)S(1)} %constant_dynamic-update-slice_fusion.2.refs_1_), channel_id=1, source_target_pairs={{0,4},{1,5},{2,6},{3,7},{4,0},{5,1},{6,2},{7,3},{8,12},{9,13},{10,... | collective-permute-start | bytes 589832 | tf_op jit(solution)/shard_map/ppermute | solution.py:144
  12.5 1.4 %collective-permute-start.12 = (bf16[48,2048]{1,0:T(8,128)(2,1)S(1)}, bf16[48,2048]{1,0:T(8,128)(2,1)S(1)}, u32[]{:S(2)}, u32[]{:S(2)}) collective-permute-start(bf16[48,2048]{1,0:T(8,128)(2,1)S(1)} %constant_dynamic-update-slice_fusion.refs_0_), channel_id=1, source_target_pairs={{0,4},{1,5},{2,6},{3,7},{4,0},{5,1},{6,2},{7,3},{8,12},{9,13},{10,... | collective-permute-start | bytes 589832 | tf_op jit(solution)/shard_map/ppermute | solution.py:144
  13.9 1.5 %collective-permute-start.6 = (bf16[48,2048]{1,0:T(8,128)(2,1)S(1)}, bf16[48,2048]{1,0:T(8,128)(2,1)S(1)}, u32[]{:S(2)}, u32[]{:S(2)}) collective-permute-start(bf16[48,2048]{1,0:T(8,128)(2,1)S(1)} %constant_dynamic-update-slice_fusion.refs_0_), channel_id=1, source_target_pairs={{0,2},{1,3},{2,0},{3,1},{4,6},{5,7},{6,4},{7,5},{8,10},{9,11},{10,... | collective-permute-start | bytes 589832 | tf_op jit(solution)/shard_map/ppermute | solution.py:144
  16.0 2.4 %collective-permute-done.13.refs_1_ = bf16[48,2048]{1,0:T(8,128)(2,1)S(1)} collective-permute-done((bf16[48,2048]{1,0:T(8,128)(2,1)S(1)}, bf16[48,2048]{1,0:T(8,128)(2,1)S(1)}, u32[]{:S(2)}, u32[]{:S(2)}) %collective-permute-start.13) | collective-permute-done | bytes 196640 | tf_op jit(solution)/shard_map/ppermute | solution.py:144
  18.4 2.1 %collective-permute-done.12.refs_0_ = bf16[48,2048]{1,0:T(8,128)(2,1)S(1)} collective-permute-done((bf16[48,2048]{1,0:T(8,128)(2,1)S(1)}, bf16[48,2048]{1,0:T(8,128)(2,1)S(1)}, u32[]{:S(2)}, u32[]{:S(2)}) %collective-permute-start.12) | collective-permute-done | bytes 196640 | tf_op jit(solution)/shard_map/ppermute | solution.py:144
  20.5 1.2 %collective-permute-done.6.refs_0_ = bf16[48,2048]{1,0:T(8,128)(2,1)S(1)} collective-permute-done((bf16[48,2048]{1,0:T(8,128)(2,1)S(1)}, bf16[48,2048]{1,0:T(8,128)(2,1)S(1)}, u32[]{:S(2)}, u32[]{:S(2)}) %collective-permute-start.6) | collective-permute-done | bytes 196640 | tf_op jit(solution)/shard_map/ppermute | solution.py:144
  21.7 2.1 %collective-permute-done.7.refs_1_ = bf16[48,2048]{1,0:T(8,128)(2,1)S(1)} collective-permute-done((bf16[48,2048]{1,0:T(8,128)(2,1)S(1)}, bf16[48,2048]{1,0:T(8,128)(2,1)S(1)}, u32[]{:S(2)}, u32[]{:S(2)}) %collective-permute-start.7) | collective-permute-done | bytes 196640 | tf_op jit(solution)/shard_map/ppermute | solution.py:144
  23.8 1.5 %collective-permute-start.19 = (bf16[48,2048]{1,0:T(8,128)(2,1)S(1)}, bf16[48,2048]{1,0:T(8,128)(2,1)S(1)}, u32[]{:S(2)}, u32[]{:S(2)}) collective-permute-start(bf16[48,2048]{1,0:T(8,128)(2,1)S(1)} %collective-permute-done.13.refs_1_), channel_id=1, source_target_pairs={{0,2},{1,3},{2,0},{3,1},{4,6},{5,7},{6,4},{7,5},{8,10},{9,11},{10,... | collective-permute-start | bytes 589832 | tf_op jit(solution)/shard_map/ppermute | solution.py:144
  25.9 1.8 %load.3.refs_6_ = bf16[704,2048]{1,0:T(8,128)(2,1)S(1)} custom-call(bf16[1,704,2048]{2,1,0:T(8,128)(2,1)} %refs_0_.1), custom_call_target="tpu_custom_call" | custom-call | tf_op jit(solution)/shard_map/load/pallas_call | solution.py:35
  27.7 2.7 %load.2 = (bf16[704,2048]{1,0:T(8,128)(2,1)S(1)}, bf16[704,2048]{1,0:T(8,128)(2,1)S(1)}) custom-call(bf16[1,704,2048]{2,1,0:T(8,128)(2,1)} %bitcast.23, bf16[1,704,2048]{2,1,0:T(8,128)(2,1)} %bitcast.24), custom_call_target="tpu_custom_call" | custom-call | tf_op jit(solution)/shard_map/load/pallas_call | solution.py:35
  31.1 2.6 %ffn.6 = (f32[96,2048]{1,0:T(8,128)S(1)}, bf16[96,2048]{1,0:T(8,128)(2,1)S(1)}) custom-call(bf16[48,2048]{1,0:T(8,128)(2,1)S(1)} %collective-permute-done.12.refs_0_, bf16[48,2048]{1,0:T(8,128)(2,1)S(1)} %collective-permute-done.13.refs_1_, bf16[48,2048]{1,0:T(8,128)(2,1)S(1)} %collective-permute-done.14.refs_2_, ...), custom_call_target="tpu_custom_call" | custom-call | flops 1660944384 | bytes 11796480 | tf_op jit(solution)/shard_map/ffn/pallas_call | solution.py:70
  34.3 2.6 %ffn.4 = (f32[96,2048]{1,0:T(8,128)S(1)}, bf16[96,2048]{1,0:T(8,128)(2,1)S(1)}) custom-call(bf16[48,2048]{1,0:T(8,128)(2,1)S(1)} %constant_dynamic-update-slice_fusion.refs_0_, bf16[48,2048]{1,0:T(8,128)(2,1)S(1)} %constant_dynamic-update-slice_fusion.2.refs_1_, bf16[48,2048]{1,0:T(8,128)(2,1)S(1)} %collective-permute-done.3.refs_2_, ...), custom_call_target="tpu_custom_call" | custom-call | flops 1660944384 | bytes 11796480 | tf_op jit(solution)/shard_map/ffn/pallas_call | solution.py:70
  37.4 2.6 %ffn.5 = (f32[96,2048]{1,0:T(8,128)S(1)}, bf16[96,2048]{1,0:T(8,128)(2,1)S(1)}) custom-call(bf16[48,2048]{1,0:T(8,128)(2,1)S(1)} %collective-permute-done.6.refs_0_, bf16[48,2048]{1,0:T(8,128)(2,1)S(1)} %collective-permute-done.7.refs_1_, bf16[48,2048]{1,0:T(8,128)(2,1)S(1)} %collective-permute-done.8.refs_2_, ...), custom_call_target="tpu_custom_call" | custom-call | flops 1660944384 | bytes 11796480 | tf_op jit(solution)/shard_map/ffn/pallas_call | solution.py:70
  40.2 2.6 %ffn.7 = (f32[96,2048]{1,0:T(8,128)S(1)}, bf16[96,2048]{1,0:T(8,128)(2,1)S(1)}) custom-call(bf16[48,2048]{1,0:T(8,128)(2,1)S(1)} %collective-permute-done.18.refs_0_, bf16[48,2048]{1,0:T(8,128)(2,1)S(1)} %collective-permute-done.19.refs_1_, bf16[48,2048]{1,0:T(8,128)(2,1)S(1)} %collective-permute-done.20.refs_2_, ...), custom_call_target="tpu_custom_call" | custom-call | flops 1660944384 | bytes 11796480 | tf_op jit(solution)/shard_map/ffn/pallas_call | solution.py:70
  43.4 1.6 %collective-permute-start.25 = (bf16[72,2048]{1,0:T(8,128)(2,1)S(1)}, bf16[72,2048]{1,0:T(8,128)(2,1)S(1)}, u32[]{:S(2)}, u32[]{:S(2)}) collective-permute-start(bf16[72,2048]{1,0:T(8,128)(2,1)S(1)} %slice.57), channel_id=1, source_target_pairs={{0,4},{1,5},{2,6},{3,7},{4,0},{5,1},{6,2},{7,3},{8,12},{9,13},{10,... | collective-permute-start | bytes 884744 | tf_op jit(solution)/shard_map/ppermute | solution.py:144
  46.3 2.5 %collective-permute-start.28 = (bf16[24,2048]{1,0:T(8,128)(2,1)S(1)}, bf16[24,2048]{1,0:T(8,128)(2,1)S(1)}, u32[]{:S(2)}, u32[]{:S(2)}) collective-permute-start(bf16[24,2048]{1,0:T(8,128)(2,1)S(1)} %get-tuple-element.33), channel_id=1, source_target_pairs={{0,6},{1,7},{2,4},{3,5},{4,2},{5,3},{6,0},{7,1},{8,14},{9,15},{10,... | collective-permute-start | bytes 294920 | tf_op jit(solution)/shard_map/ppermute | solution.py:144
  49.5 7.7 %collective-permute-done.28.arrived = bf16[24,2048]{1,0:T(8,128)(2,1)S(1)} collective-permute-done((bf16[24,2048]{1,0:T(8,128)(2,1)S(1)}, bf16[24,2048]{1,0:T(8,128)(2,1)S(1)}, u32[]{:S(2)}, u32[]{:S(2)}) %collective-permute-start.28) | collective-permute-done | bytes 98336 | tf_op jit(solution)/shard_map/ppermute | solution.py:144
  57.7 2.4 %collective-permute-start.23 = (bf16[24,2048]{1,0:T(8,128)(2,1)S(1)}, bf16[24,2048]{1,0:T(8,128)(2,1)S(1)}, u32[]{:S(2)}, u32[]{:S(2)}) collective-permute-start(bf16[24,2048]{1,0:T(8,128)(2,1)S(1)} %get-tuple-element.32), channel_id=1, source_target_pairs={{0,6},{1,7},{2,4},{3,5},{4,2},{5,3},{6,0},{7,1},{8,14},{9,15},{10,... | collective-permute-start | bytes 294920 | tf_op jit(solution)/shard_map/ppermute | solution.py:144
  60.2 4.6 %collective-permute-start.29 = (bf16[24,2048]{1,0:T(8,128)(2,1)S(1)}, bf16[24,2048]{1,0:T(8,128)(2,1)S(1)}, u32[]{:S(2)}, u32[]{:S(2)}) collective-permute-start(bf16[24,2048]{1,0:T(8,128)(2,1)S(1)} %close.3), channel_id=1, source_target_pairs={{0,16},{1,17},{2,18},{3,19},{4,20},{5,21},{6,22},{7,23},{8,24},{9,... | collective-permute-start | bytes 294920 | tf_op jit(solution)/shard_map/ppermute | solution.py:139
  64.9 1.2 %collective-permute-start.27 = (bf16[24,2048]{1,0:T(8,128)(2,1)S(1)}, bf16[24,2048]{1,0:T(8,128)(2,1)S(1)}, u32[]{:S(2)}, u32[]{:S(2)}) collective-permute-start(bf16[24,2048]{1,0:T(8,128)(2,1)S(1)} %get-tuple-element.27), channel_id=1, source_target_pairs={{0,24},{1,25},{2,26},{3,27},{4,28},{5,29},{6,30},{7,31},{8,0},{9,1... | collective-permute-start | bytes 294920 | tf_op jit(solution)/shard_map/ppermute | solution.py:139
  66.1 0.9 collective-permute-start.30
  67.0 2.6 %collective-permute-done.29 = bf16[24,2048]{1,0:T(8,128)(2,1)S(1)} collective-permute-done((bf16[24,2048]{1,0:T(8,128)(2,1)S(1)}, bf16[24,2048]{1,0:T(8,128)(2,1)S(1)}, u32[]{:S(2)}, u32[]{:S(2)}) %collective-permute-start.29) | collective-permute-done | bytes 98336 | tf_op jit(solution)/shard_map/ppermute | solution.py:139
  69.6 1.0 %collective-permute-done.27 = bf16[24,2048]{1,0:T(8,128)(2,1)S(1)} collective-permute-done((bf16[24,2048]{1,0:T(8,128)(2,1)S(1)}, bf16[24,2048]{1,0:T(8,128)(2,1)S(1)}, u32[]{:S(2)}, u32[]{:S(2)}) %collective-permute-start.27) | collective-permute-done | bytes 98336 | tf_op jit(solution)/shard_map/ppermute | solution.py:139
  70.6 2.0 %collective-permute-done.30 = bf16[24,2048]{1,0:T(8,128)(2,1)S(1)} collective-permute-done((bf16[24,2048]{1,0:T(8,128)(2,1)S(1)}, bf16[24,2048]{1,0:T(8,128)(2,1)S(1)}, u32[]{:S(2)}, u32[]{:S(2)}) %collective-permute-start.30) | collective-permute-done | bytes 98336 | tf_op jit(solution)/shard_map/ppermute | solution.py:139
  73.6 10.7 %all_to_all.5 = f32[32,1,1536]{2,1,0:T(1,128)S(1)} all-to-all(f32[32,1,1536]{2,1,0:T(1,128)S(1)} %reshape.32), channel_id=1, replica_groups=mesh['grp'=1,'ep'=32] {'ep'}, dimensions={0} | all-to-all | bytes 393216 | tf_op jit(solution)/shard_map/all_to_all | solution.py:199
  84.8 1.1 %reduce = f32[32,1536]{1,0:T(8,128)S(1)} reduce(f32[32,1,1536]{2,1,0:T(1,128)S(1)} %all_to_all.5, f32[]{:T(128)} %broadcast.35), dimensions={1}, to_apply=%all_to_all.3.reduce_sub_computation | reduce | bytes 393220 | tf_op jit(solution)/shard_map/all_to_all | solution.py:199
  86.1 0.8 copy.11
  (76 shorter events, 7.9 us)
Async XLA Ops:
  0.0 10.7 %collective-permute-start.1 = (bf16[24,2048]{1,0:T(8,128)(2,1)}, bf16[24,2048]{1,0:T(8,128)(2,1)S(1)}, u32[]{:S(2)}, u32[]{:S(2)}) collective-permute-start(bf16[24,2048]{1,0:T(8,128)(2,1)} %param.8), channel_id=1, source_target_pairs={{0,16},{1,17},{2,18},{3,19},{4,20},{5,21},{6,22},{7,23},{8,24},{9,... | collective-permute-start | bytes 294920 | tf_op jit(solution)/shard_map/ppermute | solution.py:139
  4.1 6.6 %collective-permute-start.2 = (bf16[24,2048]{1,0:T(8,128)(2,1)}, bf16[24,2048]{1,0:T(8,128)(2,1)S(1)}, u32[]{:S(2)}, u32[]{:S(2)}) collective-permute-start(bf16[24,2048]{1,0:T(8,128)(2,1)} %param.8), channel_id=1, source_target_pairs={{0,24},{1,25},{2,26},{3,27},{4,28},{5,29},{6,30},{7,31},{8,0},{9,1... | collective-permute-start | bytes 294920 | tf_op jit(solution)/shard_map/ppermute | solution.py:139
  5.4 7.1 %collective-permute-start = (bf16[24,2048]{1,0:T(8,128)(2,1)}, bf16[24,2048]{1,0:T(8,128)(2,1)S(1)}, u32[]{:S(2)}, u32[]{:S(2)}) collective-permute-start(bf16[24,2048]{1,0:T(8,128)(2,1)} %param.8), channel_id=1, source_target_pairs={{0,8},{1,9},{2,10},{3,11},{4,12},{5,13},{6,14},{7,15},{8,16},{9,17... | collective-permute-start | bytes 294920 | tf_op jit(solution)/shard_map/ppermute | solution.py:139
  10.7 7.7 %collective-permute-start.13 = (bf16[48,2048]{1,0:T(8,128)(2,1)S(1)}, bf16[48,2048]{1,0:T(8,128)(2,1)S(1)}, u32[]{:S(2)}, u32[]{:S(2)}) collective-permute-start(bf16[48,2048]{1,0:T(8,128)(2,1)S(1)} %constant_dynamic-update-slice_fusion.2.refs_1_), channel_id=1, source_target_pairs={{0,4},{1,5},{2,6},{3,7},{4,0},{5,1},{6,2},{7,3},{8,12},{9,13},{10,... | collective-permute-start | bytes 589832 | tf_op jit(solution)/shard_map/ppermute | solution.py:144
  12.5 8.0 %collective-permute-start.12 = (bf16[48,2048]{1,0:T(8,128)(2,1)S(1)}, bf16[48,2048]{1,0:T(8,128)(2,1)S(1)}, u32[]{:S(2)}, u32[]{:S(2)}) collective-permute-start(bf16[48,2048]{1,0:T(8,128)(2,1)S(1)} %constant_dynamic-update-slice_fusion.refs_0_), channel_id=1, source_target_pairs={{0,4},{1,5},{2,6},{3,7},{4,0},{5,1},{6,2},{7,3},{8,12},{9,13},{10,... | collective-permute-start | bytes 589832 | tf_op jit(solution)/shard_map/ppermute | solution.py:144
  13.9 7.8 %collective-permute-start.6 = (bf16[48,2048]{1,0:T(8,128)(2,1)S(1)}, bf16[48,2048]{1,0:T(8,128)(2,1)S(1)}, u32[]{:S(2)}, u32[]{:S(2)}) collective-permute-start(bf16[48,2048]{1,0:T(8,128)(2,1)S(1)} %constant_dynamic-update-slice_fusion.refs_0_), channel_id=1, source_target_pairs={{0,2},{1,3},{2,0},{3,1},{4,6},{5,7},{6,4},{7,5},{8,10},{9,11},{10,... | collective-permute-start | bytes 589832 | tf_op jit(solution)/shard_map/ppermute | solution.py:144
  15.4 8.4 %collective-permute-start.7 = (bf16[48,2048]{1,0:T(8,128)(2,1)S(1)}, bf16[48,2048]{1,0:T(8,128)(2,1)S(1)}, u32[]{:S(2)}, u32[]{:S(2)}) collective-permute-start(bf16[48,2048]{1,0:T(8,128)(2,1)S(1)} %constant_dynamic-update-slice_fusion.2.refs_1_), channel_id=1, source_target_pairs={{0,2},{1,3},{2,0},{3,1},{4,6},{5,7},{6,4},{7,5},{8,10},{9,11},{10,... | collective-permute-start | bytes 589832 | tf_op jit(solution)/shard_map/ppermute | solution.py:144
  16.0 9.4 %collective-permute-start.4 = (bf16[48,2048]{1,0:T(8,128)(2,1)S(1)}, bf16[48,2048]{1,0:T(8,128)(2,1)S(1)}, u32[]{:S(2)}, u32[]{:S(2)}) collective-permute-start(bf16[48,2048]{1,0:T(8,128)(2,1)S(1)} %constant_dynamic-update-slice_fusion.2.refs_1_), channel_id=1, source_target_pairs={{0,1},{1,0},{2,3},{3,2},{4,5},{5,4},{6,7},{7,6},{8,9},{9,8},{10,11... | collective-permute-start | bytes 589832 | tf_op jit(solution)/shard_map/ppermute | solution.py:144
  18.4 12.1 %collective-permute-start.15 = (bf16[48,2048]{1,0:T(8,128)(2,1)S(1)}, bf16[48,2048]{1,0:T(8,128)(2,1)S(1)}, u32[]{:S(2)}, u32[]{:S(2)}) collective-permute-start(bf16[48,2048]{1,0:T(8,128)(2,1)S(1)} %collective-permute-done.13.refs_1_), channel_id=1, source_target_pairs={{0,1},{1,0},{2,3},{3,2},{4,5},{5,4},{6,7},{7,6},{8,9},{9,8},{10,11... | collective-permute-start | bytes 589832 | tf_op jit(solution)/shard_map/ppermute | solution.py:144
  20.5 10.1 %collective-permute-start.14 = (bf16[48,2048]{1,0:T(8,128)(2,1)S(1)}, bf16[48,2048]{1,0:T(8,128)(2,1)S(1)}, u32[]{:S(2)}, u32[]{:S(2)}) collective-permute-start(bf16[48,2048]{1,0:T(8,128)(2,1)S(1)} %collective-permute-done.12.refs_0_), channel_id=1, source_target_pairs={{0,1},{1,0},{2,3},{3,2},{4,5},{5,4},{6,7},{7,6},{8,9},{9,8},{10,11... | collective-permute-start | bytes 589832 | tf_op jit(solution)/shard_map/ppermute | solution.py:144
  21.7 11.9 %collective-permute-start.3 = (bf16[48,2048]{1,0:T(8,128)(2,1)S(1)}, bf16[48,2048]{1,0:T(8,128)(2,1)S(1)}, u32[]{:S(2)}, u32[]{:S(2)}) collective-permute-start(bf16[48,2048]{1,0:T(8,128)(2,1)S(1)} %constant_dynamic-update-slice_fusion.refs_0_), channel_id=1, source_target_pairs={{0,1},{1,0},{2,3},{3,2},{4,5},{5,4},{6,7},{7,6},{8,9},{9,8},{10,11... | collective-permute-start | bytes 589832 | tf_op jit(solution)/shard_map/ppermute | solution.py:144
  23.8 10.0 %collective-permute-start.19 = (bf16[48,2048]{1,0:T(8,128)(2,1)S(1)}, bf16[48,2048]{1,0:T(8,128)(2,1)S(1)}, u32[]{:S(2)}, u32[]{:S(2)}) collective-permute-start(bf16[48,2048]{1,0:T(8,128)(2,1)S(1)} %collective-permute-done.13.refs_1_), channel_id=1, source_target_pairs={{0,2},{1,3},{2,0},{3,1},{4,6},{5,7},{6,4},{7,5},{8,10},{9,11},{10,... | collective-permute-start | bytes 589832 | tf_op jit(solution)/shard_map/ppermute | solution.py:144
  25.3 8.9 %collective-permute-start.18 = (bf16[48,2048]{1,0:T(8,128)(2,1)S(1)}, bf16[48,2048]{1,0:T(8,128)(2,1)S(1)}, u32[]{:S(2)}, u32[]{:S(2)}) collective-permute-start(bf16[48,2048]{1,0:T(8,128)(2,1)S(1)} %collective-permute-done.6.refs_0_), channel_id=1, source_target_pairs={{0,4},{1,5},{2,6},{3,7},{4,0},{5,1},{6,2},{7,3},{8,12},{9,13},{10,... | collective-permute-start | bytes 589832 | tf_op jit(solution)/shard_map/ppermute | solution.py:144
  30.5 6.4 %collective-permute-start.8 = (bf16[48,2048]{1,0:T(8,128)(2,1)S(1)}, bf16[48,2048]{1,0:T(8,128)(2,1)S(1)}, u32[]{:S(2)}, u32[]{:S(2)}) collective-permute-start(bf16[48,2048]{1,0:T(8,128)(2,1)S(1)} %collective-permute-done.6.refs_0_), channel_id=1, source_target_pairs={{0,1},{1,0},{2,3},{3,2},{4,5},{5,4},{6,7},{7,6},{8,9},{9,8},{10,11... | collective-permute-start | bytes 589832 | tf_op jit(solution)/shard_map/ppermute | solution.py:144
  30.6 6.8 %collective-permute-start.9 = (bf16[48,2048]{1,0:T(8,128)(2,1)S(1)}, bf16[48,2048]{1,0:T(8,128)(2,1)S(1)}, u32[]{:S(2)}, u32[]{:S(2)}) collective-permute-start(bf16[48,2048]{1,0:T(8,128)(2,1)S(1)} %collective-permute-done.7.refs_1_), channel_id=1, source_target_pairs={{0,1},{1,0},{2,3},{3,2},{4,5},{5,4},{6,7},{7,6},{8,9},{9,8},{10,11... | collective-permute-start | bytes 589832 | tf_op jit(solution)/shard_map/ppermute | solution.py:144
  33.7 9.6 %collective-permute-start.16 = (bf16[96,2048]{1,0:T(8,128)(2,1)S(1)}, bf16[96,2048]{1,0:T(8,128)(2,1)S(1)}, u32[]{:S(2)}, u32[]{:S(2)}) collective-permute-start(bf16[96,2048]{1,0:T(8,128)(2,1)S(1)} %get-tuple-element.24), channel_id=1, source_target_pairs={{0,1},{1,0},{2,3},{3,2},{4,5},{5,4},{6,7},{7,6},{8,9},{9,8},{10,11... | collective-permute-start | bytes 1179656 | tf_op jit(solution)/shard_map/ppermute | solution.py:144
  33.8 6.3 %collective-permute-start.21 = (bf16[48,2048]{1,0:T(8,128)(2,1)S(1)}, bf16[48,2048]{1,0:T(8,128)(2,1)S(1)}, u32[]{:S(2)}, u32[]{:S(2)}) collective-permute-start(bf16[48,2048]{1,0:T(8,128)(2,1)S(1)} %collective-permute-done.19.refs_1_), channel_id=1, source_target_pairs={{0,1},{1,0},{2,3},{3,2},{4,5},{5,4},{6,7},{7,6},{8,9},{9,8},{10,11... | collective-permute-start | bytes 589832 | tf_op jit(solution)/shard_map/ppermute | solution.py:144
  34.3 5.9 %collective-permute-start.20 = (bf16[48,2048]{1,0:T(8,128)(2,1)S(1)}, bf16[48,2048]{1,0:T(8,128)(2,1)S(1)}, u32[]{:S(2)}, u32[]{:S(2)}) collective-permute-start(bf16[48,2048]{1,0:T(8,128)(2,1)S(1)} %collective-permute-done.18.refs_0_), channel_id=1, source_target_pairs={{0,1},{1,0},{2,3},{3,2},{4,5},{5,4},{6,7},{7,6},{8,9},{9,8},{10,11... | collective-permute-start | bytes 589832 | tf_op jit(solution)/shard_map/ppermute | solution.py:144
  36.9 11.9 %collective-permute-start.5 = (bf16[96,2048]{1,0:T(8,128)(2,1)S(1)}, bf16[96,2048]{1,0:T(8,128)(2,1)S(1)}, u32[]{:S(2)}, u32[]{:S(2)}) collective-permute-start(bf16[96,2048]{1,0:T(8,128)(2,1)S(1)} %get-tuple-element.20), channel_id=1, source_target_pairs={{0,1},{1,0},{2,3},{3,2},{4,5},{5,4},{6,7},{7,6},{8,9},{9,8},{10,11... | collective-permute-start | bytes 1179656 | tf_op jit(solution)/shard_map/ppermute | solution.py:144
  40.0 4.9 %collective-permute-start.10 = (bf16[96,2048]{1,0:T(8,128)(2,1)S(1)}, bf16[96,2048]{1,0:T(8,128)(2,1)S(1)}, u32[]{:S(2)}, u32[]{:S(2)}) collective-permute-start(bf16[96,2048]{1,0:T(8,128)(2,1)S(1)} %get-tuple-element.22), channel_id=1, source_target_pairs={{0,1},{1,0},{2,3},{3,2},{4,5},{5,4},{6,7},{7,6},{8,9},{9,8},{10,11... | collective-permute-start | bytes 1179656 | tf_op jit(solution)/shard_map/ppermute | solution.py:144
  42.7 3.4 %collective-permute-start.22 = (bf16[96,2048]{1,0:T(8,128)(2,1)S(1)}, bf16[96,2048]{1,0:T(8,128)(2,1)S(1)}, u32[]{:S(2)}, u32[]{:S(2)}) collective-permute-start(bf16[96,2048]{1,0:T(8,128)(2,1)S(1)} %get-tuple-element.26), channel_id=1, source_target_pairs={{0,1},{1,0},{2,3},{3,2},{4,5},{5,4},{6,7},{7,6},{8,9},{9,8},{10,11... | collective-permute-start | bytes 1179656 | tf_op jit(solution)/shard_map/ppermute | solution.py:144
  43.4 14.3 %collective-permute-start.25 = (bf16[72,2048]{1,0:T(8,128)(2,1)S(1)}, bf16[72,2048]{1,0:T(8,128)(2,1)S(1)}, u32[]{:S(2)}, u32[]{:S(2)}) collective-permute-start(bf16[72,2048]{1,0:T(8,128)(2,1)S(1)} %slice.57), channel_id=1, source_target_pairs={{0,4},{1,5},{2,6},{3,7},{4,0},{5,1},{6,2},{7,3},{8,12},{9,13},{10,... | collective-permute-start | bytes 884744 | tf_op jit(solution)/shard_map/ppermute | solution.py:144
  45.0 15.1 %collective-permute-start.24 = (bf16[72,2048]{1,0:T(8,128)(2,1)S(1)}, bf16[72,2048]{1,0:T(8,128)(2,1)S(1)}, u32[]{:S(2)}, u32[]{:S(2)}) collective-permute-start(bf16[72,2048]{1,0:T(8,128)(2,1)S(1)} %slice.56), channel_id=1, source_target_pairs={{0,2},{1,3},{2,0},{3,1},{4,6},{5,7},{6,4},{7,5},{8,10},{9,11},{10,... | collective-permute-start | bytes 884744 | tf_op jit(solution)/shard_map/ppermute | solution.py:144
  45.6 20.5 %collective-permute-start.17 = (bf16[24,2048]{1,0:T(8,128)(2,1)S(1)}, bf16[24,2048]{1,0:T(8,128)(2,1)S(1)}, u32[]{:S(2)}, u32[]{:S(2)}) collective-permute-start(bf16[24,2048]{1,0:T(8,128)(2,1)S(1)} %slice.54), channel_id=1, source_target_pairs={{0,4},{1,5},{2,6},{3,7},{4,0},{5,1},{6,2},{7,3},{8,12},{9,13},{10,... | collective-permute-start | bytes 294920 | tf_op jit(solution)/shard_map/ppermute | solution.py:144
  46.3 26.2 %copy-start.2 = (bf16[24,2048]{1,0:T(8,128)(2,1)S(1)}, bf16[24,2048]{1,0:T(8,128)(2,1)}, u32[]{:S(2)}) copy-start(bf16[24,2048]{1,0:T(8,128)(2,1)} %param.8) | copy-start | bytes 294916
  46.3 10.9 %collective-permute-start.28 = (bf16[24,2048]{1,0:T(8,128)(2,1)S(1)}, bf16[24,2048]{1,0:T(8,128)(2,1)S(1)}, u32[]{:S(2)}, u32[]{:S(2)}) collective-permute-start(bf16[24,2048]{1,0:T(8,128)(2,1)S(1)} %get-tuple-element.33), channel_id=1, source_target_pairs={{0,6},{1,7},{2,4},{3,5},{4,2},{5,3},{6,0},{7,1},{8,14},{9,15},{10,... | collective-permute-start | bytes 294920 | tf_op jit(solution)/shard_map/ppermute | solution.py:144
  48.8 16.0 %collective-permute-start.26 = (bf16[48,2048]{1,0:T(8,128)(2,1)S(1)}, bf16[48,2048]{1,0:T(8,128)(2,1)S(1)}, u32[]{:S(2)}, u32[]{:S(2)}) collective-permute-start(bf16[48,2048]{1,0:T(8,128)(2,1)S(1)} %pad_maximum_fusion), channel_id=1, source_target_pairs={{0,6},{1,7},{2,4},{3,5},{4,2},{5,3},{6,0},{7,1},{8,14},{9,15},{10,... | collective-permute-start | bytes 589832 | tf_op jit(solution)/shard_map/ppermute | solution.py:144
  57.2 9.8 %collective-permute-start.11 = (bf16[24,2048]{1,0:T(8,128)(2,1)S(1)}, bf16[24,2048]{1,0:T(8,128)(2,1)S(1)}, u32[]{:S(2)}, u32[]{:S(2)}) collective-permute-start(bf16[24,2048]{1,0:T(8,128)(2,1)S(1)} %slice.53), channel_id=1, source_target_pairs={{0,2},{1,3},{2,0},{3,1},{4,6},{5,7},{6,4},{7,5},{8,10},{9,11},{10,... | collective-permute-start | bytes 294920 | tf_op jit(solution)/shard_map/ppermute | solution.py:144
  57.7 9.3 %collective-permute-start.23 = (bf16[24,2048]{1,0:T(8,128)(2,1)S(1)}, bf16[24,2048]{1,0:T(8,128)(2,1)S(1)}, u32[]{:S(2)}, u32[]{:S(2)}) collective-permute-start(bf16[24,2048]{1,0:T(8,128)(2,1)S(1)} %get-tuple-element.32), channel_id=1, source_target_pairs={{0,6},{1,7},{2,4},{3,5},{4,2},{5,3},{6,0},{7,1},{8,14},{9,15},{10,... | collective-permute-start | bytes 294920 | tf_op jit(solution)/shard_map/ppermute | solution.py:144
  60.2 9.4 %collective-permute-start.29 = (bf16[24,2048]{1,0:T(8,128)(2,1)S(1)}, bf16[24,2048]{1,0:T(8,128)(2,1)S(1)}, u32[]{:S(2)}, u32[]{:S(2)}) collective-permute-start(bf16[24,2048]{1,0:T(8,128)(2,1)S(1)} %close.3), channel_id=1, source_target_pairs={{0,16},{1,17},{2,18},{3,19},{4,20},{5,21},{6,22},{7,23},{8,24},{9,... | collective-permute-start | bytes 294920 | tf_op jit(solution)/shard_map/ppermute | solution.py:139
  64.9 5.7 %collective-permute-start.27 = (bf16[24,2048]{1,0:T(8,128)(2,1)S(1)}, bf16[24,2048]{1,0:T(8,128)(2,1)S(1)}, u32[]{:S(2)}, u32[]{:S(2)}) collective-permute-start(bf16[24,2048]{1,0:T(8,128)(2,1)S(1)} %get-tuple-element.27), channel_id=1, source_target_pairs={{0,24},{1,25},{2,26},{3,27},{4,28},{5,29},{6,30},{7,31},{8,0},{9,1... | collective-permute-start | bytes 294920 | tf_op jit(solution)/shard_map/ppermute | solution.py:139
  66.1 6.4 %collective-permute-start.30 = (bf16[24,2048]{1,0:T(8,128)(2,1)S(1)}, bf16[24,2048]{1,0:T(8,128)(2,1)S(1)}, u32[]{:S(2)}, u32[]{:S(2)}) collective-permute-start(bf16[24,2048]{1,0:T(8,128)(2,1)S(1)} %get-tuple-element.28), channel_id=1, source_target_pairs={{0,8},{1,9},{2,10},{3,11},{4,12},{5,13},{6,14},{7,15},{8,16},{9,17... | collective-permute-start | bytes 294920 | tf_op jit(solution)/shard_map/ppermute | solution.py:139
  (4 other events, 57.1 us)

commit v2 on v1

--- a/solution.py
+++ b/solution.py
@@ -13,34 +13,39 @@
 
 ALPHA = 8.0**0.25
 LN_EPS = 1e-05
+TN = (((0,), (0,)), ((), ()))
 CUT = 256
+CHUNKS = 4
+LANES = 128
 NT = (((1,), (1,)), ((), ()))
 
 
 def load_kernel(n, *refs):
     sources, targets, sems = refs[:n], refs[n : 2 * n], refs[2 * n]
-    copies = [
-        pltpu.make_async_copy(a.at[0], b, sems.at[i])
-        for i, (a, b) in enumerate(zip(sources, targets, strict=True))
-    ]
+    copies = []
+    for i, (source, target) in enumerate(zip(sources, targets, strict=True)):
+        step = target.shape[0] // CHUNKS if target.shape[0] % (16 * CHUNKS) == 0 else target.shape[0]
+        for c in range(target.shape[0] // step):
+            part = pl.ds(c * step, step)
+            copies.append(pltpu.make_async_copy(source.at[part], target.at[part], sems.at[i, c]))
     for copy in copies:
         copy.start()
     for copy in copies:
         copy.wait()
 
 
-def load(*weights):
-    n = len(weights)
-    weights = [pltpu.with_memory_space_constraint(w, pltpu.HBM) for w in weights]
+def load(*arrays):
+    n = len(arrays)
+    arrays = [pltpu.with_memory_space_constraint(x, pltpu.HBM) for x in arrays]
     return pl.pallas_call(
         functools.partial(load_kernel, n),
         in_specs=[pl.BlockSpec(memory_space=pltpu.HBM)] * n,
         out_specs=[pl.BlockSpec(memory_space=pltpu.VMEM)] * n,
-        out_shape=[jax.ShapeDtypeStruct(w.shape[1:], w.dtype) for w in weights],
-        scratch_shapes=[pltpu.SemaphoreType.DMA((n,))],
+        out_shape=[jax.ShapeDtypeStruct(x.shape, x.dtype) for x in arrays],
+        scratch_shapes=[pltpu.SemaphoreType.DMA((n, CHUNKS))],
         compiler_params=pltpu.CompilerParams(vmem_limit_bytes=2 << 20),
         name="load",
-    )(*weights)
+    )(*arrays)
 
 
 def ffn_kernel(n, *refs):
@@ -86,12 +91,14 @@
     )(*blocks, w_gate, w_up, w_down)
 
 
-def shares_kernel(experts, routes, gates, out):
+def shares_kernel(experts, routes, gates, out, wide):
     first = lax.div(lax.axis_index("ep"), SPAN)
+    wide[...] = jnp.zeros_like(wide)
     for k in range(experts):
         named = routes[...] == lax.rem(first + k, experts)
         share = jnp.where(named, gates[...], jnp.float32(0.0))
-        out[k : k + 1, :] = jnp.sum(share, axis=0, keepdims=True)
+        wide[k : k + 1, : routes.shape[1]] = jnp.sum(share, axis=0, keepdims=True)
+    out[...] = wide[...].T[: out.shape[0], :]
 
 
 def shares(routes, gates, experts):
@@ -100,7 +107,8 @@
         functools.partial(shares_kernel, experts),
         in_specs=[on_chip, on_chip],
         out_specs=on_chip,
-        out_shape=jax.ShapeDtypeStruct((experts, routes.shape[1]), jnp.float32),
+        out_shape=jax.ShapeDtypeStruct((routes.shape[1], SPAN), jnp.float32),
+        scratch_shapes=[pltpu.VMEM((SPAN, LANES), jnp.float32)],
         compiler_params=pltpu.CompilerParams(vmem_limit_bytes=2 << 20),
         name="shares",
     )(routes, gates)
@@ -127,11 +135,77 @@
     )(base, *parts, arrived)
 
 
+def norm_kernel(n, devices, *refs):
+    tokens, base, weight = refs[:3]
+    stays, backs, out = refs[3 : 3 + n], refs[3 + n : -1], refs[-1]
+    rows, width = tokens.shape
+    columns = width // devices
+    per_lane_row = LANES // columns
+    mine = base[:rows, :]
+    for part in stays:
+        mine = mine + part[...].astype(jnp.float32)
+    z = ALPHA * tokens[...].astype(jnp.float32) + weight[:, :1] * mine
+    for k, part in enumerate(backs):
+        z = z + weight[:, k + 1 : k + 2] * part[...].astype(jnp.float32)
+    mean = jnp.sum(z, axis=1, keepdims=True) / width
+    var = jnp.sum(z * z, axis=1, keepdims=True) / width - mean * mean
+    normed = (z - mean) * lax.rsqrt(var + LN_EPS)
+    deep = rows // per_lane_row
+    for d in range(devices):
+        piece = normed[:, d * columns : (d + 1) * columns]
+        piece = [piece[h * deep : (h + 1) * deep] for h in range(per_lane_row)]
+        out[d * deep : (d + 1) * deep, :] = jnp.concatenate(piece, axis=1)
+
+
+def norm(tokens, base, weight, stays, backs, devices):
+    rows, width = tokens.shape
+    on_chip = pl.BlockSpec(memory_space=pltpu.VMEM)
+    args = (tokens, base, weight, *stays, *backs)
+    return pl.pallas_call(
+        functools.partial(norm_kernel, len(stays), devices),
+        in_specs=[on_chip] * len(args),
+        out_specs=on_chip,
+        out_shape=jax.ShapeDtypeStruct((rows * width // LANES, LANES), jnp.float32),
+        compiler_params=pltpu.CompilerParams(vmem_limit_bytes=8 << 20),
+        name="norm",
+    )(*args)
+
+
+def finish_kernel(deep, x, gain, bias, out):
+    packed, lanes = x.shape
+    columns, tokens = out.shape
+    y = (x[...] * gain[...] + bias[...]).astype(jnp.bfloat16)
+    spot = lax.broadcasted_iota(jnp.int32, (packed, 1), 0)
+    spot = spot + lax.div(spot, deep) * (deep * (lanes // columns - 1))
+    lane = lax.broadcasted_iota(jnp.int32, (packed, tokens), 1)
+    total = jnp.zeros(out.shape, jnp.float32)
+    for h in range(lanes // columns):
+        place = jnp.where(lane == spot + h * deep, 1.0, 0.0).astype(jnp.bfloat16)
+        total = total + lax.dot_general(
+            y[:, h * columns : (h + 1) * columns], place, TN, preferred_element_type=jnp.float32
+        )
+    out[...] = total.astype(jnp.bfloat16)
+
+
+def finish(x, rows, gain, bias):
+    columns = gain.shape[0]
+    fold = LANES // columns
+    on_chip = pl.BlockSpec(memory_space=pltpu.VMEM)
+    wide = lambda v: jnp.concatenate([v] * fold).reshape(1, LANES)
+    return pl.pallas_call(
+        functools.partial(finish_kernel, rows // fold),
+        in_specs=[on_chip] * 3,
+        out_specs=on_chip,
+        out_shape=jax.ShapeDtypeStruct((columns, x.size // columns), jnp.bfloat16),
+        compiler_params=pltpu.CompilerParams(vmem_limit_bytes=8 << 20),
+        name="finish",
+    )(x, wide(gain), wide(bias))
+
+
 def on_device(tokens, routes, gates, w_gate, w_up, w_down, norm_gain, norm_bias):
-    rows, width = tokens.shape
+    rows, _ = tokens.shape
     devices = lax.axis_size("ep")
     experts = devices // SPAN
-    columns = width // devices
     peers = list(range(2, SPAN, 2))
     others = range(1, experts)
 
@@ -143,15 +217,15 @@
     def across(x, m):
         return lax.ppermute(x, "ep", [(i, i ^ m) for i in range(devices)])
 
-    projections = load(w_gate.transpose(0, 2, 1), w_up.transpose(0, 2, 1))
-    weights = (*projections, *load(w_down))
+    *projections, held = load(w_gate[0].T, w_up[0].T, tokens)
+    weights = (*projections, *load(w_down[0]))
 
     def run(own):
         other = [across(x, 1) for x in own]
         kept, given = ffn(own, other, *weights)
         return kept + across(given, 1).astype(jnp.float32)
 
-    blocks = [tokens] + [along(tokens, k) for k in others]
+    blocks = [held] + [along(tokens, k) for k in others]
     half = experts // 2
     first, second, far = peers
     early = jnp.concatenate(blocks[:half], axis=0)
@@ -170,9 +244,7 @@
 
     summed = {
         m: run(halves).astype(jnp.bfloat16)
-        for m, halves in (
-            (first, remote[first]), (second, remote[second]), (far, (upper, lower))
-        )
+        for m, halves in ((first, remote[first]), (second, remote[second]), (far, (upper, lower)))
     }
     put = {m: across(summed[m][rows:], m) for m in (first, second)}
     put_lead = across(pick(summed[far], ahead), far)
@@ -183,21 +255,12 @@
         sums = close(ks, rows, result, [put[first], put[second]], arrived)
         for k, total in zip(ks, sums, strict=True):
             back[k] = along(total, -k)
-    mine = result[:rows]
-    for m in peers:
-        mine = mine + across(summed[m][:rows], m).astype(jnp.float32)
+    stays = [across(summed[m][:rows], m) for m in peers]
 
     weight = shares(routes.T, gates.T, experts)
-
-    z = ALPHA * tokens.astype(jnp.float32) + weight[0][:, None] * mine
-    for k in others:
-        z = z + weight[k][:, None] * back[k].astype(jnp.float32)
-    mean = jnp.mean(z, axis=1, keepdims=True)
-    var = jnp.mean(z * z, axis=1, keepdims=True) - mean * mean
-    normed = (z - mean) * lax.rsqrt(var + LN_EPS)
-    normed = normed.reshape(rows, devices, columns).transpose(1, 0, 2)
-    normed = lax.all_to_all(normed, "ep", 0, 0, tiled=True).reshape(devices * rows, columns)
-    return (normed * norm_gain[None, :] + norm_bias[None, :]).astype(jnp.bfloat16)
+    packed = norm(held, result, weight, stays, [back[k] for k in others], devices)
+    packed = lax.all_to_all(packed.reshape(devices, 1, -1), "ep", 0, 0, tiled=True)
+    return finish(packed.reshape(-1, LANES), rows, norm_gain, norm_bias).T
 
 
 def solution(mesh):

time: 87.1 us -> 83.8 us (0.962)
  blocking collectives: 10.7 us -> 0 us
  waiting for transfers between devices: 24.8 us -> 32.1 us
  local copies, waits for them, and re-layouts: 3.11 us -> 0.14 us
  Pallas kernels: 15 us -> 17.2 us
  starting transfers between devices: 31.1 us -> 33.3 us
  other arithmetic: 1.84 us -> 0.41 us
    all_to_all x1 -> x0, blocking collectives: 10.7 us -> none  [on_device(): lax.all_to_all(normed, 'ep', 0, 0, tiled=True)]
    all_to_all x0 -> x1, waiting for transfers between devices: none -> 8.85 us  [on_device(): lax.all_to_all(packed.reshape(devices, 1, -1), 'ep', 0, 0, tiled=True)]
    all_to_all x0 -> x1, starting transfers between devices: none -> 2.58 us  [on_device(): lax.all_to_all(packed.reshape(devices, 1, -1), 'ep', 0, 0, tiled=True)]
    pallas_call x0 -> x2, Pallas kernels: none -> 2.16 us  [the longest x1 1.1 us: finish(): pl.pallas_call(functools.partial(finish_kernel, rows // fold), in_specs=[...]
    ppermute x6, waiting for transfers between devices: 9.21 us -> 7.39 us  [along(): lax.ppermute(x, 'ep', [(i, (i + k * SPAN) % devices) for i in range(devic...]
    unnamed x14 -> x10, local copies, waits for them, and re-layouts: 1.32 us -> 0.04 us
    all_to_all x1 -> x0, other arithmetic: 1.1 us -> none  [on_device(): lax.all_to_all(normed, 'ep', 0, 0, tiled=True)]
  transfers between devices with their start and end apart: 31 -> 32, of which waited for: 9 -> 10; matrix products, arithmetic and copies ran while one was open for 2% -> 1% of each run, Pallas kernels for 17% -> 18%
where the time goes in v2:
time: 83.8 us; the launch traced here: 83.6 us
  starting transfers between devices  33.3 us (40%)
  waiting for transfers between devices  32.1 us (38%)
  Pallas kernels  17.2 us (21%)
    ppermute x25, starting transfers between devices, across(): return lax.ppermute(x, 'ep', [(i, i ^ m) for i in range(devices)])  18.7 us
    ppermute x25, waiting for transfers between devices, across(): return lax.ppermute(x, 'ep', [(i, i ^ m) for i in range(devices)])  15.9 us
    ppermute x6, starting transfers between devices, along(): lax.ppermute(x, 'ep', [(i, (i + k * SPAN) % devices) for i in range(devic...  12.1 us
    pallas_call x4, Pallas kernels, ffn(): pl.pallas_call(functools.partial(ffn_kernel, len(blocks)), in_specs=[on_c...  10.3 us
    all_to_all x1, waiting for transfers between devices, on_device(): lax.all_to_all(packed.reshape(devices, 1, -1), 'ep', 0, 0, tiled=True)  8.85 us
    ppermute x6, waiting for transfers between devices, along(): lax.ppermute(x, 'ep', [(i, (i + k * SPAN) % devices) for i in range(devic...  7.39 us
    pallas_call x2, Pallas kernels, load(): pl.pallas_call(functools.partial(load_kernel, n), in_specs=[pl.BlockSpec(...  4.53 us
    all_to_all x1, starting transfers between devices, on_device(): lax.all_to_all(packed.reshape(devices, 1, -1), 'ep', 0, 0, tiled=True)  2.58 us
  transfers between devices with their start and end apart: 32, of which 10 were waited for; matrix products, arithmetic and copies ran while one was open for 1% of the time, Pallas kernels for 18%

profile of v2, /device:TPU:0, one launch (start us, length us, event | category | flops | bytes accessed | tf_op | source)
XLA Modules:
  0.0 83.6 jit_solution(8644902772991606652)
XLA Ops:
  0.0 3.1 %collective-permute-start = (bf16[24,2048]{1,0:T(8,128)(2,1)}, bf16[24,2048]{1,0:T(8,128)(2,1)S(1)}, u32[]{:S(2)}, u32[]{:S(2)}) collective-permute-start(bf16[24,2048]{1,0:T(8,128)(2,1)} %refs_2_.1), channel_id=1, source_target_pairs={{0,8},{1,9},{2,10},{3,11},{4,12},{5,13},{6,14},{7,15},{8,16},{9,17... | collective-permute-start | bytes 294920 | tf_op jit(solution)/shard_map/ppermute | solution.py:213
  3.1 2.6 %collective-permute-start.1 = (bf16[24,2048]{1,0:T(8,128)(2,1)}, bf16[24,2048]{1,0:T(8,128)(2,1)S(1)}, u32[]{:S(2)}, u32[]{:S(2)}) collective-permute-start(bf16[24,2048]{1,0:T(8,128)(2,1)} %refs_2_.1), channel_id=1, source_target_pairs={{0,16},{1,17},{2,18},{3,19},{4,20},{5,21},{6,22},{7,23},{8,24},{9,... | collective-permute-start | bytes 294920 | tf_op jit(solution)/shard_map/ppermute | solution.py:213
  5.6 1.3 %collective-permute-start.2 = (bf16[24,2048]{1,0:T(8,128)(2,1)}, bf16[24,2048]{1,0:T(8,128)(2,1)S(1)}, u32[]{:S(2)}, u32[]{:S(2)}) collective-permute-start(bf16[24,2048]{1,0:T(8,128)(2,1)} %refs_2_.1), channel_id=1, source_target_pairs={{0,24},{1,25},{2,26},{3,27},{4,28},{5,29},{6,30},{7,31},{8,0},{9,1... | collective-permute-start | bytes 294920 | tf_op jit(solution)/shard_map/ppermute | solution.py:213
  7.0 2.7 %load.2 = (bf16[704,2048]{1,0:T(8,128)(2,1)S(1)}, bf16[704,2048]{1,0:T(8,128)(2,1)S(1)}, bf16[24,2048]{1,0:T(8,128)(2,1)S(1)}) custom-call(bf16[704,2048]{1,0:T(8,128)(2,1)} %bitcast.19, bf16[704,2048]{1,0:T(8,128)(2,1)} %bitcast.20, bf16[24,2048]{1,0:T(8,128)(2,1)} %refs_2_.1), custom_call_target="tpu_custom_call" | custom-call | tf_op jit(solution)/shard_map/load/pallas_call | solution.py:40
  9.8 1.6 %collective-permute-start.12 = (bf16[48,2048]{1,0:T(8,128)(2,1)S(1)}, bf16[48,2048]{1,0:T(8,128)(2,1)S(1)}, u32[]{:S(2)}, u32[]{:S(2)}) collective-permute-start(bf16[48,2048]{1,0:T(8,128)(2,1)S(1)} %constant_dynamic-update-slice_fusion.refs_0_), channel_id=1, source_target_pairs={{0,4},{1,5},{2,6},{3,7},{4,0},{5,1},{6,2},{7,3},{8,12},{9,13},{10,... | collective-permute-start | bytes 589832 | tf_op jit(solution)/shard_map/ppermute | solution.py:218
  11.4 1.1 %collective-permute-done.1 = bf16[24,2048]{1,0:T(8,128)(2,1)S(1)} collective-permute-done((bf16[24,2048]{1,0:T(8,128)(2,1)}, bf16[24,2048]{1,0:T(8,128)(2,1)S(1)}, u32[]{:S(2)}, u32[]{:S(2)}) %collective-permute-start.1) | collective-permute-done | bytes 98336 | tf_op jit(solution)/shard_map/ppermute | solution.py:213
  12.5 1.6 %collective-permute-start.13 = (bf16[48,2048]{1,0:T(8,128)(2,1)S(1)}, bf16[48,2048]{1,0:T(8,128)(2,1)S(1)}, u32[]{:S(2)}, u32[]{:S(2)}) collective-permute-start(bf16[48,2048]{1,0:T(8,128)(2,1)S(1)} %constant_dynamic-update-slice_fusion.2.refs_1_), channel_id=1, source_target_pairs={{0,4},{1,5},{2,6},{3,7},{4,0},{5,1},{6,2},{7,3},{8,12},{9,13},{10,... | collective-permute-start | bytes 589832 | tf_op jit(solution)/shard_map/ppermute | solution.py:218
  14.1 1.5 %collective-permute-start.6 = (bf16[48,2048]{1,0:T(8,128)(2,1)S(1)}, bf16[48,2048]{1,0:T(8,128)(2,1)S(1)}, u32[]{:S(2)}, u32[]{:S(2)}) collective-permute-start(bf16[48,2048]{1,0:T(8,128)(2,1)S(1)} %constant_dynamic-update-slice_fusion.refs_0_), channel_id=1, source_target_pairs={{0,2},{1,3},{2,0},{3,1},{4,6},{5,7},{6,4},{7,5},{8,10},{9,11},{10,... | collective-permute-start | bytes 589832 | tf_op jit(solution)/shard_map/ppermute | solution.py:218
  15.6 0.5 collective-permute-start.7
  16.6 3.2 %collective-permute-done.13.refs_1_ = bf16[48,2048]{1,0:T(8,128)(2,1)S(1)} collective-permute-done((bf16[48,2048]{1,0:T(8,128)(2,1)S(1)}, bf16[48,2048]{1,0:T(8,128)(2,1)S(1)}, u32[]{:S(2)}, u32[]{:S(2)}) %collective-permute-start.13) | collective-permute-done | bytes 196640 | tf_op jit(solution)/shard_map/ppermute | solution.py:218
  19.9 2.0 %collective-permute-done.6.refs_0_ = bf16[48,2048]{1,0:T(8,128)(2,1)S(1)} collective-permute-done((bf16[48,2048]{1,0:T(8,128)(2,1)S(1)}, bf16[48,2048]{1,0:T(8,128)(2,1)S(1)}, u32[]{:S(2)}, u32[]{:S(2)}) %collective-permute-start.6) | collective-permute-done | bytes 196640 | tf_op jit(solution)/shard_map/ppermute | solution.py:218
  21.9 2.9 %collective-permute-done.7.refs_1_ = bf16[48,2048]{1,0:T(8,128)(2,1)S(1)} collective-permute-done((bf16[48,2048]{1,0:T(8,128)(2,1)S(1)}, bf16[48,2048]{1,0:T(8,128)(2,1)S(1)}, u32[]{:S(2)}, u32[]{:S(2)}) %collective-permute-start.7) | collective-permute-done | bytes 196640 | tf_op jit(solution)/shard_map/ppermute | solution.py:218
  25.2 1.5 %collective-permute-start.19 = (bf16[48,2048]{1,0:T(8,128)(2,1)S(1)}, bf16[48,2048]{1,0:T(8,128)(2,1)S(1)}, u32[]{:S(2)}, u32[]{:S(2)}) collective-permute-start(bf16[48,2048]{1,0:T(8,128)(2,1)S(1)} %collective-permute-done.13.refs_1_), channel_id=1, source_target_pairs={{0,2},{1,3},{2,0},{3,1},{4,6},{5,7},{6,4},{7,5},{8,10},{9,11},{10,... | collective-permute-start | bytes 589832 | tf_op jit(solution)/shard_map/ppermute | solution.py:218
  26.7 1.8 %load.3.refs_6_ = bf16[704,2048]{1,0:T(8,128)(2,1)S(1)} custom-call(bf16[704,2048]{1,0:T(8,128)(2,1)} %bitcast.21), custom_call_target="tpu_custom_call" | custom-call | tf_op jit(solution)/shard_map/load/pallas_call | solution.py:40
  29.1 2.6 %ffn.6 = (f32[96,2048]{1,0:T(8,128)S(1)}, bf16[96,2048]{1,0:T(8,128)(2,1)S(1)}) custom-call(bf16[48,2048]{1,0:T(8,128)(2,1)S(1)} %collective-permute-done.12.refs_0_, bf16[48,2048]{1,0:T(8,128)(2,1)S(1)} %collective-permute-done.13.refs_1_, bf16[48,2048]{1,0:T(8,128)(2,1)S(1)} %collective-permute-done.14.refs_2_, ...), custom_call_target="tpu_custom_call" | custom-call | flops 1660944384 | bytes 11796480 | tf_op jit(solution)/shard_map/ffn/pallas_call | solution.py:75
  32.4 2.6 %ffn.4 = (f32[96,2048]{1,0:T(8,128)S(1)}, bf16[96,2048]{1,0:T(8,128)(2,1)S(1)}) custom-call(bf16[48,2048]{1,0:T(8,128)(2,1)S(1)} %constant_dynamic-update-slice_fusion.refs_0_, bf16[48,2048]{1,0:T(8,128)(2,1)S(1)} %constant_dynamic-update-slice_fusion.2.refs_1_, bf16[48,2048]{1,0:T(8,128)(2,1)S(1)} %collective-permute-done.3.refs_2_, ...), custom_call_target="tpu_custom_call" | custom-call | flops 1660944384 | bytes 11796480 | tf_op jit(solution)/shard_map/ffn/pallas_call | solution.py:75
  35.4 2.6 %ffn.5 = (f32[96,2048]{1,0:T(8,128)S(1)}, bf16[96,2048]{1,0:T(8,128)(2,1)S(1)}) custom-call(bf16[48,2048]{1,0:T(8,128)(2,1)S(1)} %collective-permute-done.6.refs_0_, bf16[48,2048]{1,0:T(8,128)(2,1)S(1)} %collective-permute-done.7.refs_1_, bf16[48,2048]{1,0:T(8,128)(2,1)S(1)} %collective-permute-done.8.refs_2_, ...), custom_call_target="tpu_custom_call" | custom-call | flops 1660944384 | bytes 11796480 | tf_op jit(solution)/shard_map/ffn/pallas_call | solution.py:75
  38.2 2.6 %ffn.7 = (f32[96,2048]{1,0:T(8,128)S(1)}, bf16[96,2048]{1,0:T(8,128)(2,1)S(1)}) custom-call(bf16[48,2048]{1,0:T(8,128)(2,1)S(1)} %collective-permute-done.18.refs_0_, bf16[48,2048]{1,0:T(8,128)(2,1)S(1)} %collective-permute-done.19.refs_1_, bf16[48,2048]{1,0:T(8,128)(2,1)S(1)} %collective-permute-done.20.refs_2_, ...), custom_call_target="tpu_custom_call" | custom-call | flops 1660944384 | bytes 11796480 | tf_op jit(solution)/shard_map/ffn/pallas_call | solution.py:75
  41.4 1.6 %collective-permute-start.25 = (bf16[72,2048]{1,0:T(8,128)(2,1)S(1)}, bf16[72,2048]{1,0:T(8,128)(2,1)S(1)}, u32[]{:S(2)}, u32[]{:S(2)}) collective-permute-start(bf16[72,2048]{1,0:T(8,128)(2,1)S(1)} %slice.36), channel_id=1, source_target_pairs={{0,4},{1,5},{2,6},{3,7},{4,0},{5,1},{6,2},{7,3},{8,12},{9,13},{10,... | collective-permute-start | bytes 884744 | tf_op jit(solution)/shard_map/ppermute | solution.py:218
  43.1 0.6 collective-permute-start.24
  44.4 2.5 %collective-permute-start.28 = (bf16[24,2048]{1,0:T(8,128)(2,1)S(1)}, bf16[24,2048]{1,0:T(8,128)(2,1)S(1)}, u32[]{:S(2)}, u32[]{:S(2)}) collective-permute-start(bf16[24,2048]{1,0:T(8,128)(2,1)S(1)} %get-tuple-element.31), channel_id=1, source_target_pairs={{0,6},{1,7},{2,4},{3,5},{4,2},{5,3},{6,0},{7,1},{8,14},{9,15},{10,... | collective-permute-start | bytes 294920 | tf_op jit(solution)/shard_map/ppermute | solution.py:218
  46.9 0.5 collective-permute-start.26
  47.6 7.6 %collective-permute-done.28.arrived = bf16[24,2048]{1,0:T(8,128)(2,1)S(1)} collective-permute-done((bf16[24,2048]{1,0:T(8,128)(2,1)S(1)}, bf16[24,2048]{1,0:T(8,128)(2,1)S(1)}, u32[]{:S(2)}, u32[]{:S(2)}) %collective-permute-start.28) | collective-permute-done | bytes 98336 | tf_op jit(solution)/shard_map/ppermute | solution.py:218
  55.7 2.5 %collective-permute-start.23 = (bf16[24,2048]{1,0:T(8,128)(2,1)S(1)}, bf16[24,2048]{1,0:T(8,128)(2,1)S(1)}, u32[]{:S(2)}, u32[]{:S(2)}) collective-permute-start(bf16[24,2048]{1,0:T(8,128)(2,1)S(1)} %get-tuple-element.34), channel_id=1, source_target_pairs={{0,6},{1,7},{2,4},{3,5},{4,2},{5,3},{6,0},{7,1},{8,14},{9,15},{10,... | collective-permute-start | bytes 294920 | tf_op jit(solution)/shard_map/ppermute | solution.py:218
  58.2 1.7 %collective-permute-start.29 = (bf16[24,2048]{1,0:T(8,128)(2,1)S(1)}, bf16[24,2048]{1,0:T(8,128)(2,1)S(1)}, u32[]{:S(2)}, u32[]{:S(2)}) collective-permute-start(bf16[24,2048]{1,0:T(8,128)(2,1)S(1)} %close.3), channel_id=1, source_target_pairs={{0,16},{1,17},{2,18},{3,19},{4,20},{5,21},{6,22},{7,23},{8,24},{9,... | collective-permute-start | bytes 294920 | tf_op jit(solution)/shard_map/ppermute | solution.py:213
  60.0 3.4 %collective-permute-start.27 = (bf16[24,2048]{1,0:T(8,128)(2,1)S(1)}, bf16[24,2048]{1,0:T(8,128)(2,1)S(1)}, u32[]{:S(2)}, u32[]{:S(2)}) collective-permute-start(bf16[24,2048]{1,0:T(8,128)(2,1)S(1)} %get-tuple-element.29), channel_id=1, source_target_pairs={{0,24},{1,25},{2,26},{3,27},{4,28},{5,29},{6,30},{7,31},{8,0},{9,1... | collective-permute-start | bytes 294920 | tf_op jit(solution)/shard_map/ppermute | solution.py:213
  64.1 2.1 %collective-permute-done.27.refs_6_ = bf16[24,2048]{1,0:T(8,128)(2,1)S(1)} collective-permute-done((bf16[24,2048]{1,0:T(8,128)(2,1)S(1)}, bf16[24,2048]{1,0:T(8,128)(2,1)S(1)}, u32[]{:S(2)}, u32[]{:S(2)}) %collective-permute-start.27) | collective-permute-done | bytes 98336 | tf_op jit(solution)/shard_map/ppermute | solution.py:213
  66.1 3.7 %collective-permute-done.30.refs_8_ = bf16[24,2048]{1,0:T(8,128)(2,1)S(1)} collective-permute-done((bf16[24,2048]{1,0:T(8,128)(2,1)S(1)}, bf16[24,2048]{1,0:T(8,128)(2,1)S(1)}, u32[]{:S(2)}, u32[]{:S(2)}) %collective-permute-start.30) | collective-permute-done | bytes 98336 | tf_op jit(solution)/shard_map/ppermute | solution.py:213
  69.9 1.1 %norm.1 = f32[384,128]{1,0:T(8,128)} custom-call(bf16[24,2048]{1,0:T(8,128)(2,1)S(1)} %get-tuple-element.18.refs_0_, f32[96,2048]{1,0:T(8,128)S(1)} %convert_add_fusion.base.refs_1_, f32[24,8]{1,0:T(8,128)S(1)} %shares.1.refs_2_, bf16[24,2048]{1,0:T(8,128)(2,1)S(1)} %collective-permute-done.11.refs_3_, bf16[24,2048]{1,0:T(8,128)(2,1)S(1)} %collective-permute-done.17.refs_4_, ...), custom_call_target="tpu_custom_call" | custom-call | tf_op jit(solution)/shard_map/norm/pallas_call | solution.py:164
  70.9 2.6 %all-to-all-start = ((f32[32,1,1536]{2,1,0:T(1,128)}), f32[32,1,1536]{2,1,0:T(1,128)S(1)}, u32[]{:S(2)}, u32[]{:S(2)}) async-start(f32[32,1,1536]{2,1,0:T(1,128)} %bitcast.7), calls=%async_computation | async-start | bytes 393216 | tf_op jit(solution)/shard_map/all_to_all | solution.py:262
  73.6 8.9 %all-to-all-done = f32[32,1,1536]{2,1,0:T(1,128)S(1)} async-done(((f32[32,1,1536]{2,1,0:T(1,128)}), f32[32,1,1536]{2,1,0:T(1,128)S(1)}, u32[]{:S(2)}, u32[]{:S(2)}) %all-to-all-start) | async-done | bytes 196640 | tf_op jit(solution)/shard_map/all_to_all | solution.py:262
  82.5 1.1 %finish.1 = bf16[64,768]{1,0:T(8,128)(2,1)} custom-call(f32[384,128]{1,0:T(8,128)S(1)} %bitcast.16, f32[1,128]{1,0:T(1,128)S(1)} %get-tuple-element.35.gain, f32[1,128]{1,0:T(1,128)S(1)} %get-tuple-element.36.bias), custom_call_target="tpu_custom_call" | custom-call | tf_op jit(solution)/shard_map/finish/pallas_call | solution.py:195
  (66 shorter events, 5.8 us)
Async XLA Ops:
  0.0 9.8 %collective-permute-start = (bf16[24,2048]{1,0:T(8,128)(2,1)}, bf16[24,2048]{1,0:T(8,128)(2,1)S(1)}, u32[]{:S(2)}, u32[]{:S(2)}) collective-permute-start(bf16[24,2048]{1,0:T(8,128)(2,1)} %refs_2_.1), channel_id=1, source_target_pairs={{0,8},{1,9},{2,10},{3,11},{4,12},{5,13},{6,14},{7,15},{8,16},{9,17... | collective-permute-start | bytes 294920 | tf_op jit(solution)/shard_map/ppermute | solution.py:213
  3.1 9.4 %collective-permute-start.1 = (bf16[24,2048]{1,0:T(8,128)(2,1)}, bf16[24,2048]{1,0:T(8,128)(2,1)S(1)}, u32[]{:S(2)}, u32[]{:S(2)}) collective-permute-start(bf16[24,2048]{1,0:T(8,128)(2,1)} %refs_2_.1), channel_id=1, source_target_pairs={{0,16},{1,17},{2,18},{3,19},{4,20},{5,21},{6,22},{7,23},{8,24},{9,... | collective-permute-start | bytes 294920 | tf_op jit(solution)/shard_map/ppermute | solution.py:213
  5.6 6.8 %collective-permute-start.2 = (bf16[24,2048]{1,0:T(8,128)(2,1)}, bf16[24,2048]{1,0:T(8,128)(2,1)S(1)}, u32[]{:S(2)}, u32[]{:S(2)}) collective-permute-start(bf16[24,2048]{1,0:T(8,128)(2,1)} %refs_2_.1), channel_id=1, source_target_pairs={{0,24},{1,25},{2,26},{3,27},{4,28},{5,29},{6,30},{7,31},{8,0},{9,1... | collective-permute-start | bytes 294920 | tf_op jit(solution)/shard_map/ppermute | solution.py:213
  9.8 6.5 %collective-permute-start.12 = (bf16[48,2048]{1,0:T(8,128)(2,1)S(1)}, bf16[48,2048]{1,0:T(8,128)(2,1)S(1)}, u32[]{:S(2)}, u32[]{:S(2)}) collective-permute-start(bf16[48,2048]{1,0:T(8,128)(2,1)S(1)} %constant_dynamic-update-slice_fusion.refs_0_), channel_id=1, source_target_pairs={{0,4},{1,5},{2,6},{3,7},{4,0},{5,1},{6,2},{7,3},{8,12},{9,13},{10,... | collective-permute-start | bytes 589832 | tf_op jit(solution)/shard_map/ppermute | solution.py:218
  12.5 7.4 %collective-permute-start.13 = (bf16[48,2048]{1,0:T(8,128)(2,1)S(1)}, bf16[48,2048]{1,0:T(8,128)(2,1)S(1)}, u32[]{:S(2)}, u32[]{:S(2)}) collective-permute-start(bf16[48,2048]{1,0:T(8,128)(2,1)S(1)} %constant_dynamic-update-slice_fusion.2.refs_1_), channel_id=1, source_target_pairs={{0,4},{1,5},{2,6},{3,7},{4,0},{5,1},{6,2},{7,3},{8,12},{9,13},{10,... | collective-permute-start | bytes 589832 | tf_op jit(solution)/shard_map/ppermute | solution.py:218
  14.1 7.8 %collective-permute-start.6 = (bf16[48,2048]{1,0:T(8,128)(2,1)S(1)}, bf16[48,2048]{1,0:T(8,128)(2,1)S(1)}, u32[]{:S(2)}, u32[]{:S(2)}) collective-permute-start(bf16[48,2048]{1,0:T(8,128)(2,1)S(1)} %constant_dynamic-update-slice_fusion.refs_0_), channel_id=1, source_target_pairs={{0,2},{1,3},{2,0},{3,1},{4,6},{5,7},{6,4},{7,5},{8,10},{9,11},{10,... | collective-permute-start | bytes 589832 | tf_op jit(solution)/shard_map/ppermute | solution.py:218
  15.6 9.2 %collective-permute-start.7 = (bf16[48,2048]{1,0:T(8,128)(2,1)S(1)}, bf16[48,2048]{1,0:T(8,128)(2,1)S(1)}, u32[]{:S(2)}, u32[]{:S(2)}) collective-permute-start(bf16[48,2048]{1,0:T(8,128)(2,1)S(1)} %constant_dynamic-update-slice_fusion.2.refs_1_), channel_id=1, source_target_pairs={{0,2},{1,3},{2,0},{3,1},{4,6},{5,7},{6,4},{7,5},{8,10},{9,11},{10,... | collective-permute-start | bytes 589832 | tf_op jit(solution)/shard_map/ppermute | solution.py:218
  16.1 9.1 %collective-permute-start.3 = (bf16[48,2048]{1,0:T(8,128)(2,1)S(1)}, bf16[48,2048]{1,0:T(8,128)(2,1)S(1)}, u32[]{:S(2)}, u32[]{:S(2)}) collective-permute-start(bf16[48,2048]{1,0:T(8,128)(2,1)S(1)} %constant_dynamic-update-slice_fusion.refs_0_), channel_id=1, source_target_pairs={{0,1},{1,0},{2,3},{3,2},{4,5},{5,4},{6,7},{7,6},{8,9},{9,8},{10,11... | collective-permute-start | bytes 589832 | tf_op jit(solution)/shard_map/ppermute | solution.py:218
  16.2 12.3 %collective-permute-start.14 = (bf16[48,2048]{1,0:T(8,128)(2,1)S(1)}, bf16[48,2048]{1,0:T(8,128)(2,1)S(1)}, u32[]{:S(2)}, u32[]{:S(2)}) collective-permute-start(bf16[48,2048]{1,0:T(8,128)(2,1)S(1)} %collective-permute-done.12.refs_0_), channel_id=1, source_target_pairs={{0,1},{1,0},{2,3},{3,2},{4,5},{5,4},{6,7},{7,6},{8,9},{9,8},{10,11... | collective-permute-start | bytes 589832 | tf_op jit(solution)/shard_map/ppermute | solution.py:218
  19.9 8.8 %collective-permute-start.15 = (bf16[48,2048]{1,0:T(8,128)(2,1)S(1)}, bf16[48,2048]{1,0:T(8,128)(2,1)S(1)}, u32[]{:S(2)}, u32[]{:S(2)}) collective-permute-start(bf16[48,2048]{1,0:T(8,128)(2,1)S(1)} %collective-permute-done.13.refs_1_), channel_id=1, source_target_pairs={{0,1},{1,0},{2,3},{3,2},{4,5},{5,4},{6,7},{7,6},{8,9},{9,8},{10,11... | collective-permute-start | bytes 589832 | tf_op jit(solution)/shard_map/ppermute | solution.py:218
  21.9 9.8 %collective-permute-start.4 = (bf16[48,2048]{1,0:T(8,128)(2,1)S(1)}, bf16[48,2048]{1,0:T(8,128)(2,1)S(1)}, u32[]{:S(2)}, u32[]{:S(2)}) collective-permute-start(bf16[48,2048]{1,0:T(8,128)(2,1)S(1)} %constant_dynamic-update-slice_fusion.2.refs_1_), channel_id=1, source_target_pairs={{0,1},{1,0},{2,3},{3,2},{4,5},{5,4},{6,7},{7,6},{8,9},{9,8},{10,11... | collective-permute-start | bytes 589832 | tf_op jit(solution)/shard_map/ppermute | solution.py:218
  24.7 7.1 %collective-permute-start.18 = (bf16[48,2048]{1,0:T(8,128)(2,1)S(1)}, bf16[48,2048]{1,0:T(8,128)(2,1)S(1)}, u32[]{:S(2)}, u32[]{:S(2)}) collective-permute-start(bf16[48,2048]{1,0:T(8,128)(2,1)S(1)} %collective-permute-done.6.refs_0_), channel_id=1, source_target_pairs={{0,4},{1,5},{2,6},{3,7},{4,0},{5,1},{6,2},{7,3},{8,12},{9,13},{10,... | collective-permute-start | bytes 589832 | tf_op jit(solution)/shard_map/ppermute | solution.py:218
  25.2 7.1 %collective-permute-start.19 = (bf16[48,2048]{1,0:T(8,128)(2,1)S(1)}, bf16[48,2048]{1,0:T(8,128)(2,1)S(1)}, u32[]{:S(2)}, u32[]{:S(2)}) collective-permute-start(bf16[48,2048]{1,0:T(8,128)(2,1)S(1)} %collective-permute-done.13.refs_1_), channel_id=1, source_target_pairs={{0,2},{1,3},{2,0},{3,1},{4,6},{5,7},{6,4},{7,5},{8,10},{9,11},{10,... | collective-permute-start | bytes 589832 | tf_op jit(solution)/shard_map/ppermute | solution.py:218
  28.5 6.4 %collective-permute-start.8 = (bf16[48,2048]{1,0:T(8,128)(2,1)S(1)}, bf16[48,2048]{1,0:T(8,128)(2,1)S(1)}, u32[]{:S(2)}, u32[]{:S(2)}) collective-permute-start(bf16[48,2048]{1,0:T(8,128)(2,1)S(1)} %collective-permute-done.6.refs_0_), channel_id=1, source_target_pairs={{0,1},{1,0},{2,3},{3,2},{4,5},{5,4},{6,7},{7,6},{8,9},{9,8},{10,11... | collective-permute-start | bytes 589832 | tf_op jit(solution)/shard_map/ppermute | solution.py:218
  28.6 6.8 %collective-permute-start.9 = (bf16[48,2048]{1,0:T(8,128)(2,1)S(1)}, bf16[48,2048]{1,0:T(8,128)(2,1)S(1)}, u32[]{:S(2)}, u32[]{:S(2)}) collective-permute-start(bf16[48,2048]{1,0:T(8,128)(2,1)S(1)} %collective-permute-done.7.refs_1_), channel_id=1, source_target_pairs={{0,1},{1,0},{2,3},{3,2},{4,5},{5,4},{6,7},{7,6},{8,9},{9,8},{10,11... | collective-permute-start | bytes 589832 | tf_op jit(solution)/shard_map/ppermute | solution.py:218
  31.7 9.6 %collective-permute-start.16 = (bf16[96,2048]{1,0:T(8,128)(2,1)S(1)}, bf16[96,2048]{1,0:T(8,128)(2,1)S(1)}, u32[]{:S(2)}, u32[]{:S(2)}) collective-permute-start(bf16[96,2048]{1,0:T(8,128)(2,1)S(1)} %get-tuple-element.26), channel_id=1, source_target_pairs={{0,1},{1,0},{2,3},{3,2},{4,5},{5,4},{6,7},{7,6},{8,9},{9,8},{10,11... | collective-permute-start | bytes 1179656 | tf_op jit(solution)/shard_map/ppermute | solution.py:218
  31.9 6.3 %collective-permute-start.20 = (bf16[48,2048]{1,0:T(8,128)(2,1)S(1)}, bf16[48,2048]{1,0:T(8,128)(2,1)S(1)}, u32[]{:S(2)}, u32[]{:S(2)}) collective-permute-start(bf16[48,2048]{1,0:T(8,128)(2,1)S(1)} %collective-permute-done.18.refs_0_), channel_id=1, source_target_pairs={{0,1},{1,0},{2,3},{3,2},{4,5},{5,4},{6,7},{7,6},{8,9},{9,8},{10,11... | collective-permute-start | bytes 589832 | tf_op jit(solution)/shard_map/ppermute | solution.py:218
  32.3 5.9 %collective-permute-start.21 = (bf16[48,2048]{1,0:T(8,128)(2,1)S(1)}, bf16[48,2048]{1,0:T(8,128)(2,1)S(1)}, u32[]{:S(2)}, u32[]{:S(2)}) collective-permute-start(bf16[48,2048]{1,0:T(8,128)(2,1)S(1)} %collective-permute-done.19.refs_1_), channel_id=1, source_target_pairs={{0,1},{1,0},{2,3},{3,2},{4,5},{5,4},{6,7},{7,6},{8,9},{9,8},{10,11... | collective-permute-start | bytes 589832 | tf_op jit(solution)/shard_map/ppermute | solution.py:218
  35.0 11.9 %collective-permute-start.5 = (bf16[96,2048]{1,0:T(8,128)(2,1)S(1)}, bf16[96,2048]{1,0:T(8,128)(2,1)S(1)}, u32[]{:S(2)}, u32[]{:S(2)}) collective-permute-start(bf16[96,2048]{1,0:T(8,128)(2,1)S(1)} %get-tuple-element.22), channel_id=1, source_target_pairs={{0,1},{1,0},{2,3},{3,2},{4,5},{5,4},{6,7},{7,6},{8,9},{9,8},{10,11... | collective-permute-start | bytes 1179656 | tf_op jit(solution)/shard_map/ppermute | solution.py:218
  38.0 5.0 %collective-permute-start.10 = (bf16[96,2048]{1,0:T(8,128)(2,1)S(1)}, bf16[96,2048]{1,0:T(8,128)(2,1)S(1)}, u32[]{:S(2)}, u32[]{:S(2)}) collective-permute-start(bf16[96,2048]{1,0:T(8,128)(2,1)S(1)} %get-tuple-element.24), channel_id=1, source_target_pairs={{0,1},{1,0},{2,3},{3,2},{4,5},{5,4},{6,7},{7,6},{8,9},{9,8},{10,11... | collective-permute-start | bytes 1179656 | tf_op jit(solution)/shard_map/ppermute | solution.py:218
  40.8 3.4 %collective-permute-start.22 = (bf16[96,2048]{1,0:T(8,128)(2,1)S(1)}, bf16[96,2048]{1,0:T(8,128)(2,1)S(1)}, u32[]{:S(2)}, u32[]{:S(2)}) collective-permute-start(bf16[96,2048]{1,0:T(8,128)(2,1)S(1)} %get-tuple-element.28), channel_id=1, source_target_pairs={{0,1},{1,0},{2,3},{3,2},{4,5},{5,4},{6,7},{7,6},{8,9},{9,8},{10,11... | collective-permute-start | bytes 1179656 | tf_op jit(solution)/shard_map/ppermute | solution.py:218
  41.4 14.3 %collective-permute-start.25 = (bf16[72,2048]{1,0:T(8,128)(2,1)S(1)}, bf16[72,2048]{1,0:T(8,128)(2,1)S(1)}, u32[]{:S(2)}, u32[]{:S(2)}) collective-permute-start(bf16[72,2048]{1,0:T(8,128)(2,1)S(1)} %slice.36), channel_id=1, source_target_pairs={{0,4},{1,5},{2,6},{3,7},{4,0},{5,1},{6,2},{7,3},{8,12},{9,13},{10,... | collective-permute-start | bytes 884744 | tf_op jit(solution)/shard_map/ppermute | solution.py:218
  43.1 15.1 %collective-permute-start.24 = (bf16[72,2048]{1,0:T(8,128)(2,1)S(1)}, bf16[72,2048]{1,0:T(8,128)(2,1)S(1)}, u32[]{:S(2)}, u32[]{:S(2)}) collective-permute-start(bf16[72,2048]{1,0:T(8,128)(2,1)S(1)} %slice.35), channel_id=1, source_target_pairs={{0,2},{1,3},{2,0},{3,1},{4,6},{5,7},{6,4},{7,5},{8,10},{9,11},{10,... | collective-permute-start | bytes 884744 | tf_op jit(solution)/shard_map/ppermute | solution.py:218
  43.7 19.8 %collective-permute-start.17 = (bf16[24,2048]{1,0:T(8,128)(2,1)S(1)}, bf16[24,2048]{1,0:T(8,128)(2,1)S(1)}, u32[]{:S(2)}, u32[]{:S(2)}) collective-permute-start(bf16[24,2048]{1,0:T(8,128)(2,1)S(1)} %slice.33), channel_id=1, source_target_pairs={{0,4},{1,5},{2,6},{3,7},{4,0},{5,1},{6,2},{7,3},{8,12},{9,13},{10,... | collective-permute-start | bytes 294920 | tf_op jit(solution)/shard_map/ppermute | solution.py:218
  44.4 10.8 %collective-permute-start.28 = (bf16[24,2048]{1,0:T(8,128)(2,1)S(1)}, bf16[24,2048]{1,0:T(8,128)(2,1)S(1)}, u32[]{:S(2)}, u32[]{:S(2)}) collective-permute-start(bf16[24,2048]{1,0:T(8,128)(2,1)S(1)} %get-tuple-element.31), channel_id=1, source_target_pairs={{0,6},{1,7},{2,4},{3,5},{4,2},{5,3},{6,0},{7,1},{8,14},{9,15},{10,... | collective-permute-start | bytes 294920 | tf_op jit(solution)/shard_map/ppermute | solution.py:218
  46.9 13.0 %collective-permute-start.26 = (bf16[48,2048]{1,0:T(8,128)(2,1)S(1)}, bf16[48,2048]{1,0:T(8,128)(2,1)S(1)}, u32[]{:S(2)}, u32[]{:S(2)}) collective-permute-start(bf16[48,2048]{1,0:T(8,128)(2,1)S(1)} %pad_maximum_fusion), channel_id=1, source_target_pairs={{0,6},{1,7},{2,4},{3,5},{4,2},{5,3},{6,0},{7,1},{8,14},{9,15},{10,... | collective-permute-start | bytes 589832 | tf_op jit(solution)/shard_map/ppermute | solution.py:218
  55.2 8.4 %collective-permute-start.11 = (bf16[24,2048]{1,0:T(8,128)(2,1)S(1)}, bf16[24,2048]{1,0:T(8,128)(2,1)S(1)}, u32[]{:S(2)}, u32[]{:S(2)}) collective-permute-start(bf16[24,2048]{1,0:T(8,128)(2,1)S(1)} %slice.32), channel_id=1, source_target_pairs={{0,2},{1,3},{2,0},{3,1},{4,6},{5,7},{6,4},{7,5},{8,10},{9,11},{10,... | collective-permute-start | bytes 294920 | tf_op jit(solution)/shard_map/ppermute | solution.py:218
  55.7 7.9 %collective-permute-start.23 = (bf16[24,2048]{1,0:T(8,128)(2,1)S(1)}, bf16[24,2048]{1,0:T(8,128)(2,1)S(1)}, u32[]{:S(2)}, u32[]{:S(2)}) collective-permute-start(bf16[24,2048]{1,0:T(8,128)(2,1)S(1)} %get-tuple-element.34), channel_id=1, source_target_pairs={{0,6},{1,7},{2,4},{3,5},{4,2},{5,3},{6,0},{7,1},{8,14},{9,15},{10,... | collective-permute-start | bytes 294920 | tf_op jit(solution)/shard_map/ppermute | solution.py:218
  58.2 5.8 %collective-permute-start.29 = (bf16[24,2048]{1,0:T(8,128)(2,1)S(1)}, bf16[24,2048]{1,0:T(8,128)(2,1)S(1)}, u32[]{:S(2)}, u32[]{:S(2)}) collective-permute-start(bf16[24,2048]{1,0:T(8,128)(2,1)S(1)} %close.3), channel_id=1, source_target_pairs={{0,16},{1,17},{2,18},{3,19},{4,20},{5,21},{6,22},{7,23},{8,24},{9,... | collective-permute-start | bytes 294920 | tf_op jit(solution)/shard_map/ppermute | solution.py:213
  60.0 6.1 %collective-permute-start.27 = (bf16[24,2048]{1,0:T(8,128)(2,1)S(1)}, bf16[24,2048]{1,0:T(8,128)(2,1)S(1)}, u32[]{:S(2)}, u32[]{:S(2)}) collective-permute-start(bf16[24,2048]{1,0:T(8,128)(2,1)S(1)} %get-tuple-element.29), channel_id=1, source_target_pairs={{0,24},{1,25},{2,26},{3,27},{4,28},{5,29},{6,30},{7,31},{8,0},{9,1... | collective-permute-start | bytes 294920 | tf_op jit(solution)/shard_map/ppermute | solution.py:213
  63.4 6.4 %collective-permute-start.30 = (bf16[24,2048]{1,0:T(8,128)(2,1)S(1)}, bf16[24,2048]{1,0:T(8,128)(2,1)S(1)}, u32[]{:S(2)}, u32[]{:S(2)}) collective-permute-start(bf16[24,2048]{1,0:T(8,128)(2,1)S(1)} %get-tuple-element.30), channel_id=1, source_target_pairs={{0,8},{1,9},{2,10},{3,11},{4,12},{5,13},{6,14},{7,15},{8,16},{9,17... | collective-permute-start | bytes 294920 | tf_op jit(solution)/shard_map/ppermute | solution.py:213
  70.9 11.5 %all-to-all-start = ((f32[32,1,1536]{2,1,0:T(1,128)}), f32[32,1,1536]{2,1,0:T(1,128)S(1)}, u32[]{:S(2)}, u32[]{:S(2)}) async-start(f32[32,1,1536]{2,1,0:T(1,128)} %bitcast.7), calls=%async_computation | async-start | bytes 393216 | tf_op jit(solution)/shard_map/all_to_all | solution.py:262
  (4 other events, 90.2 us)

commit v3 on v2

--- a/solution.py
+++ b/solution.py
@@ -17,7 +17,6 @@
 CUT = 256
 CHUNKS = 4
 LANES = 128
-NT = (((1,), (1,)), ((), ()))
 
 
 def load_kernel(n, *refs):
@@ -48,14 +47,37 @@
     )(*arrays)
 
 
+def turn_kernel(n, *refs):
+    for source, target in zip(refs[:n], refs[n:], strict=True):
+        hid, width = source.shape
+        whole = hid // LANES * LANES
+        for j in range(0, width, CUT):
+            rows = slice(j, min(j + CUT, width))
+            target[rows, :whole] = source[:whole, rows].T
+            if whole < hid:
+                target[rows, whole:] = source[whole:, rows].T
+
+
+def turn(*arrays):
+    on_chip = pl.BlockSpec(memory_space=pltpu.VMEM)
+    return pl.pallas_call(
+        functools.partial(turn_kernel, len(arrays)),
+        in_specs=[on_chip] * len(arrays),
+        out_specs=[on_chip] * len(arrays),
+        out_shape=[jax.ShapeDtypeStruct(x.shape[::-1], x.dtype) for x in arrays],
+        compiler_params=pltpu.CompilerParams(vmem_limit_bytes=4 << 20),
+        name="turn",
+    )(*arrays)
+
+
 def ffn_kernel(n, *refs):
     blocks, (wg, wu, wd, kept, given, hidden) = refs[:n], refs[n:]
-    hid, width = wg.shape
+    width, hid = wg.shape
     x = jnp.concatenate([b[...] for b in blocks], axis=0)
     for j in range(0, hid, CUT):
         cols = slice(j, min(j + CUT, hid))
-        g = lax.dot_general(x, wg[cols, :], NT, preferred_element_type=jnp.float32)
-        u = lax.dot_general(x, wu[cols, :], NT, preferred_element_type=jnp.float32)
+        g = jnp.dot(x, wg[:, cols], preferred_element_type=jnp.float32)
+        u = jnp.dot(x, wu[:, cols], preferred_element_type=jnp.float32)
         hidden[:, cols] = (g / (1.0 + jnp.exp(-g)) * u).astype(jnp.bfloat16)
     split = kept.shape[0]
     h = hidden[...]
@@ -67,7 +89,7 @@
 
 
 def ffn(own, other, w_gate, w_up, w_down):
-    hid, width = w_gate.shape
+    width, hid = w_gate.shape
     n_own, n_other = (sum(b.shape[0] for b in group) for group in (own, other))
     total = n_own + n_other
     blocks = [*own, *other]
@@ -95,7 +117,7 @@
     first = lax.div(lax.axis_index("ep"), SPAN)
     wide[...] = jnp.zeros_like(wide)
     for k in range(experts):
-        named = routes[...] == lax.rem(first + k, experts)
+        named = routes[...] == lax.bitwise_xor(first, k)
         share = jnp.where(named, gates[...], jnp.float32(0.0))
         wide[k : k + 1, : routes.shape[1]] = jnp.sum(share, axis=0, keepdims=True)
     out[...] = wide[...].T[: out.shape[0], :]
@@ -210,14 +232,13 @@
     others = range(1, experts)
 
     def along(x, k):
-        return lax.ppermute(
-            x, "ep", [(i, (i + k * SPAN) % devices) for i in range(devices)]
-        )
+        return lax.ppermute(x, "ep", [(i, i ^ (k * SPAN)) for i in range(devices)])
 
     def across(x, m):
         return lax.ppermute(x, "ep", [(i, i ^ m) for i in range(devices)])
 
     *projections, held = load(w_gate[0].T, w_up[0].T, tokens)
+    projections = turn(*projections)
     weights = (*projections, *load(w_down[0]))
 
     def run(own):
@@ -254,7 +275,7 @@
     for ks, arrived in ((ahead, put_lead), (behind, put_tail)):
         sums = close(ks, rows, result, [put[first], put[second]], arrived)
         for k, total in zip(ks, sums, strict=True):
-            back[k] = along(total, -k)
+            back[k] = along(total, k)
     stays = [across(summed[m][:rows], m) for m in peers]
 
     weight = shares(routes.T, gates.T, experts)

time: 83.8 us -> 82.4 us (0.983)
  waiting for transfers between devices: 32.1 us -> 30.2 us
  starting transfers between devices: 33.3 us -> 34.5 us
    pallas_call x4, Pallas kernels: 10.3 us -> 8.03 us  [ffn(): pl.pallas_call(functools.partial(ffn_kernel, len(blocks)), in_specs=[on_c...]
    ppermute x25, waiting for transfers between devices: 15.9 us -> 13.9 us  [across(): return lax.ppermute(x, 'ep', [(i, i ^ m) for i in range(devices)])]
    pallas_call x0 -> x1, Pallas kernels: none -> 1.69 us  [turn(): pl.pallas_call(functools.partial(turn_kernel, len(arrays)), in_specs=[on_...]
    all_to_all x1, starting transfers between devices: 2.58 us -> 3.65 us  [on_device(): lax.all_to_all(packed.reshape(devices, 1, -1), 'ep', 0, 0, tiled=True)]
  transfers between devices with their start and end apart: 32 -> 32, of which waited for: 10 -> 9; matrix products, arithmetic and copies ran while one was open for 1% -> 1% of each run, Pallas kernels for 18% -> 18%
where the time goes in v3:
time: 82.4 us; the launch traced here: 82.2 us
  starting transfers between devices  34.5 us (42%)
  waiting for transfers between devices  30.2 us (37%)
  Pallas kernels  16.6 us (20%)
    ppermute x25, starting transfers between devices, across(): return lax.ppermute(x, 'ep', [(i, i ^ m) for i in range(devices)])  19 us
    ppermute x25, waiting for transfers between devices, across(): return lax.ppermute(x, 'ep', [(i, i ^ m) for i in range(devices)])  13.9 us
    ppermute x6, starting transfers between devices, along(): return lax.ppermute(x, 'ep', [(i, i ^ k * SPAN) for i in range(devices)])  11.9 us
    all_to_all x1, waiting for transfers between devices, on_device(): lax.all_to_all(packed.reshape(devices, 1, -1), 'ep', 0, 0, tiled=True)  8.85 us
    pallas_call x4, Pallas kernels, ffn(): pl.pallas_call(functools.partial(ffn_kernel, len(blocks)), in_specs=[on_c...  8.03 us
    ppermute x6, waiting for transfers between devices, along(): return lax.ppermute(x, 'ep', [(i, i ^ k * SPAN) for i in range(devices)])  7.46 us
    pallas_call x2, Pallas kernels, load(): pl.pallas_call(functools.partial(load_kernel, n), in_specs=[pl.BlockSpec(...  4.53 us
    all_to_all x1, starting transfers between devices, on_device(): lax.all_to_all(packed.reshape(devices, 1, -1), 'ep', 0, 0, tiled=True)  3.65 us
  transfers between devices with their start and end apart: 32, of which 9 were waited for; matrix products, arithmetic and copies ran while one was open for 1% of the time, Pallas kernels for 18%

profile of v3, /device:TPU:0, one launch (start us, length us, event | category | flops | bytes accessed | tf_op | source)
XLA Modules:
  0.0 82.2 jit_solution(17311348027913668418)
XLA Ops:
  0.0 3.1 %collective-permute-start = (bf16[24,2048]{1,0:T(8,128)(2,1)}, bf16[24,2048]{1,0:T(8,128)(2,1)S(1)}, u32[]{:S(2)}, u32[]{:S(2)}) collective-permute-start(bf16[24,2048]{1,0:T(8,128)(2,1)} %refs_2_.1), channel_id=1, source_target_pairs={{0,8},{1,9},{2,10},{3,11},{4,12},{5,13},{6,14},{7,15},{8,0},{9,1},... | collective-permute-start | bytes 294920 | tf_op jit(solution)/shard_map/ppermute | solution.py:235
  3.1 2.6 %collective-permute-start.1 = (bf16[24,2048]{1,0:T(8,128)(2,1)}, bf16[24,2048]{1,0:T(8,128)(2,1)S(1)}, u32[]{:S(2)}, u32[]{:S(2)}) collective-permute-start(bf16[24,2048]{1,0:T(8,128)(2,1)} %refs_2_.1), channel_id=1, source_target_pairs={{0,16},{1,17},{2,18},{3,19},{4,20},{5,21},{6,22},{7,23},{8,24},{9,... | collective-permute-start | bytes 294920 | tf_op jit(solution)/shard_map/ppermute | solution.py:235
  5.6 2.7 %load.2 = (bf16[704,2048]{1,0:T(8,128)(2,1)S(1)}, bf16[704,2048]{1,0:T(8,128)(2,1)S(1)}, bf16[24,2048]{1,0:T(8,128)(2,1)S(1)}) custom-call(bf16[704,2048]{1,0:T(8,128)(2,1)} %bitcast.19, bf16[704,2048]{1,0:T(8,128)(2,1)} %bitcast.20, bf16[24,2048]{1,0:T(8,128)(2,1)} %refs_2_.1), custom_call_target="tpu_custom_call" | custom-call | tf_op jit(solution)/shard_map/load/pallas_call | solution.py:39
  8.4 1.8 %collective-permute-start.12 = (bf16[48,2048]{1,0:T(8,128)(2,1)S(1)}, bf16[48,2048]{1,0:T(8,128)(2,1)S(1)}, u32[]{:S(2)}, u32[]{:S(2)}) collective-permute-start(bf16[48,2048]{1,0:T(8,128)(2,1)S(1)} %constant_dynamic-update-slice_fusion.refs_0_), channel_id=1, source_target_pairs={{0,4},{1,5},{2,6},{3,7},{4,0},{5,1},{6,2},{7,3},{8,12},{9,13},{10,... | collective-permute-start | bytes 589832 | tf_op jit(solution)/shard_map/ppermute | solution.py:238
  10.2 3.5 %collective-permute-done.1 = bf16[24,2048]{1,0:T(8,128)(2,1)S(1)} collective-permute-done((bf16[24,2048]{1,0:T(8,128)(2,1)}, bf16[24,2048]{1,0:T(8,128)(2,1)S(1)}, u32[]{:S(2)}, u32[]{:S(2)}) %collective-permute-start.1) | collective-permute-done | bytes 98336 | tf_op jit(solution)/shard_map/ppermute | solution.py:235
  13.7 1.6 %collective-permute-start.13 = (bf16[48,2048]{1,0:T(8,128)(2,1)S(1)}, bf16[48,2048]{1,0:T(8,128)(2,1)S(1)}, u32[]{:S(2)}, u32[]{:S(2)}) collective-permute-start(bf16[48,2048]{1,0:T(8,128)(2,1)S(1)} %constant_dynamic-update-slice_fusion.2.refs_1_), channel_id=1, source_target_pairs={{0,4},{1,5},{2,6},{3,7},{4,0},{5,1},{6,2},{7,3},{8,12},{9,13},{10,... | collective-permute-start | bytes 589832 | tf_op jit(solution)/shard_map/ppermute | solution.py:238
  15.3 1.5 %collective-permute-start.6 = (bf16[48,2048]{1,0:T(8,128)(2,1)S(1)}, bf16[48,2048]{1,0:T(8,128)(2,1)S(1)}, u32[]{:S(2)}, u32[]{:S(2)}) collective-permute-start(bf16[48,2048]{1,0:T(8,128)(2,1)S(1)} %constant_dynamic-update-slice_fusion.refs_0_), channel_id=1, source_target_pairs={{0,2},{1,3},{2,0},{3,1},{4,6},{5,7},{6,4},{7,5},{8,10},{9,11},{10,... | collective-permute-start | bytes 589832 | tf_op jit(solution)/shard_map/ppermute | solution.py:238
  16.8 0.5 collective-permute-start.7
  17.9 1.6 %collective-permute-done.13.refs_1_ = bf16[48,2048]{1,0:T(8,128)(2,1)S(1)} collective-permute-done((bf16[48,2048]{1,0:T(8,128)(2,1)S(1)}, bf16[48,2048]{1,0:T(8,128)(2,1)S(1)}, u32[]{:S(2)}, u32[]{:S(2)}) %collective-permute-start.13) | collective-permute-done | bytes 196640 | tf_op jit(solution)/shard_map/ppermute | solution.py:238
  19.5 2.5 %collective-permute-done.6.refs_0_ = bf16[48,2048]{1,0:T(8,128)(2,1)S(1)} collective-permute-done((bf16[48,2048]{1,0:T(8,128)(2,1)S(1)}, bf16[48,2048]{1,0:T(8,128)(2,1)S(1)}, u32[]{:S(2)}, u32[]{:S(2)}) %collective-permute-start.6) | collective-permute-done | bytes 196640 | tf_op jit(solution)/shard_map/ppermute | solution.py:238
  21.9 2.1 %collective-permute-done.7.refs_1_ = bf16[48,2048]{1,0:T(8,128)(2,1)S(1)} collective-permute-done((bf16[48,2048]{1,0:T(8,128)(2,1)S(1)}, bf16[48,2048]{1,0:T(8,128)(2,1)S(1)}, u32[]{:S(2)}, u32[]{:S(2)}) %collective-permute-start.7) | collective-permute-done | bytes 196640 | tf_op jit(solution)/shard_map/ppermute | solution.py:238
  24.6 1.5 %collective-permute-start.19 = (bf16[48,2048]{1,0:T(8,128)(2,1)S(1)}, bf16[48,2048]{1,0:T(8,128)(2,1)S(1)}, u32[]{:S(2)}, u32[]{:S(2)}) collective-permute-start(bf16[48,2048]{1,0:T(8,128)(2,1)S(1)} %collective-permute-done.13.refs_1_), channel_id=1, source_target_pairs={{0,2},{1,3},{2,0},{3,1},{4,6},{5,7},{6,4},{7,5},{8,10},{9,11},{10,... | collective-permute-start | bytes 589832 | tf_op jit(solution)/shard_map/ppermute | solution.py:238
  26.1 1.8 %load.3.refs_6_ = bf16[704,2048]{1,0:T(8,128)(2,1)S(1)} custom-call(bf16[704,2048]{1,0:T(8,128)(2,1)} %bitcast.21), custom_call_target="tpu_custom_call" | custom-call | tf_op jit(solution)/shard_map/load/pallas_call | solution.py:39
  27.9 1.7 %turn.1 = (bf16[2048,704]{1,0:T(8,128)(2,1)S(1)}, bf16[2048,704]{1,0:T(8,128)(2,1)S(1)}) custom-call(bf16[704,2048]{1,0:T(8,128)(2,1)S(1)} %get-tuple-element.21.refs_0_, bf16[704,2048]{1,0:T(8,128)(2,1)S(1)} %get-tuple-element.22.refs_1_), custom_call_target="tpu_custom_call" | custom-call | tf_op jit(solution)/shard_map/turn/pallas_call | solution.py:63
  30.1 2.0 %ffn.6 = (f32[96,2048]{1,0:T(8,128)S(1)}, bf16[96,2048]{1,0:T(8,128)(2,1)S(1)}) custom-call(bf16[48,2048]{1,0:T(8,128)(2,1)S(1)} %collective-permute-done.12.refs_0_, bf16[48,2048]{1,0:T(8,128)(2,1)S(1)} %collective-permute-done.13.refs_1_, bf16[48,2048]{1,0:T(8,128)(2,1)S(1)} %collective-permute-done.14.refs_2_, ...), custom_call_target="tpu_custom_call" | custom-call | flops 1660944384 | bytes 11796480 | tf_op jit(solution)/shard_map/ffn/pallas_call | solution.py:97
  32.8 2.0 %ffn.4 = (f32[96,2048]{1,0:T(8,128)S(1)}, bf16[96,2048]{1,0:T(8,128)(2,1)S(1)}) custom-call(bf16[48,2048]{1,0:T(8,128)(2,1)S(1)} %constant_dynamic-update-slice_fusion.refs_0_, bf16[48,2048]{1,0:T(8,128)(2,1)S(1)} %constant_dynamic-update-slice_fusion.2.refs_1_, bf16[48,2048]{1,0:T(8,128)(2,1)S(1)} %collective-permute-done.3.refs_2_, ...), custom_call_target="tpu_custom_call" | custom-call | flops 1660944384 | bytes 11796480 | tf_op jit(solution)/shard_map/ffn/pallas_call | solution.py:97
  35.4 2.0 %ffn.5 = (f32[96,2048]{1,0:T(8,128)S(1)}, bf16[96,2048]{1,0:T(8,128)(2,1)S(1)}) custom-call(bf16[48,2048]{1,0:T(8,128)(2,1)S(1)} %collective-permute-done.6.refs_0_, bf16[48,2048]{1,0:T(8,128)(2,1)S(1)} %collective-permute-done.7.refs_1_, bf16[48,2048]{1,0:T(8,128)(2,1)S(1)} %collective-permute-done.8.refs_2_, ...), custom_call_target="tpu_custom_call" | custom-call | flops 1660944384 | bytes 11796480 | tf_op jit(solution)/shard_map/ffn/pallas_call | solution.py:97
  37.5 2.0 %ffn.7 = (f32[96,2048]{1,0:T(8,128)S(1)}, bf16[96,2048]{1,0:T(8,128)(2,1)S(1)}) custom-call(bf16[48,2048]{1,0:T(8,128)(2,1)S(1)} %collective-permute-done.18.refs_0_, bf16[48,2048]{1,0:T(8,128)(2,1)S(1)} %collective-permute-done.19.refs_1_, bf16[48,2048]{1,0:T(8,128)(2,1)S(1)} %collective-permute-done.20.refs_2_, ...), custom_call_target="tpu_custom_call" | custom-call | flops 1660944384 | bytes 11796480 | tf_op jit(solution)/shard_map/ffn/pallas_call | solution.py:97
  40.2 1.6 %collective-permute-start.25 = (bf16[72,2048]{1,0:T(8,128)(2,1)S(1)}, bf16[72,2048]{1,0:T(8,128)(2,1)S(1)}, u32[]{:S(2)}, u32[]{:S(2)}) collective-permute-start(bf16[72,2048]{1,0:T(8,128)(2,1)S(1)} %slice.36), channel_id=1, source_target_pairs={{0,4},{1,5},{2,6},{3,7},{4,0},{5,1},{6,2},{7,3},{8,12},{9,13},{10,... | collective-permute-start | bytes 884744 | tf_op jit(solution)/shard_map/ppermute | solution.py:238
  41.9 0.6 collective-permute-start.24
  43.1 2.5 %collective-permute-start.28 = (bf16[24,2048]{1,0:T(8,128)(2,1)S(1)}, bf16[24,2048]{1,0:T(8,128)(2,1)S(1)}, u32[]{:S(2)}, u32[]{:S(2)}) collective-permute-start(bf16[24,2048]{1,0:T(8,128)(2,1)S(1)} %get-tuple-element.35), channel_id=1, source_target_pairs={{0,6},{1,7},{2,4},{3,5},{4,2},{5,3},{6,0},{7,1},{8,14},{9,15},{10,... | collective-permute-start | bytes 294920 | tf_op jit(solution)/shard_map/ppermute | solution.py:238
  45.7 0.5 collective-permute-start.26
  46.3 7.6 %collective-permute-done.28.arrived = bf16[24,2048]{1,0:T(8,128)(2,1)S(1)} collective-permute-done((bf16[24,2048]{1,0:T(8,128)(2,1)S(1)}, bf16[24,2048]{1,0:T(8,128)(2,1)S(1)}, u32[]{:S(2)}, u32[]{:S(2)}) %collective-permute-start.28) | collective-permute-done | bytes 98336 | tf_op jit(solution)/shard_map/ppermute | solution.py:238
  54.5 2.5 %collective-permute-start.23 = (bf16[24,2048]{1,0:T(8,128)(2,1)S(1)}, bf16[24,2048]{1,0:T(8,128)(2,1)S(1)}, u32[]{:S(2)}, u32[]{:S(2)}) collective-permute-start(bf16[24,2048]{1,0:T(8,128)(2,1)S(1)} %get-tuple-element.38), channel_id=1, source_target_pairs={{0,6},{1,7},{2,4},{3,5},{4,2},{5,3},{6,0},{7,1},{8,14},{9,15},{10,... | collective-permute-start | bytes 294920 | tf_op jit(solution)/shard_map/ppermute | solution.py:238
  57.0 3.7 %collective-permute-start.29 = (bf16[24,2048]{1,0:T(8,128)(2,1)S(1)}, bf16[24,2048]{1,0:T(8,128)(2,1)S(1)}, u32[]{:S(2)}, u32[]{:S(2)}) collective-permute-start(bf16[24,2048]{1,0:T(8,128)(2,1)S(1)} %close.3), channel_id=1, source_target_pairs={{0,16},{1,17},{2,18},{3,19},{4,20},{5,21},{6,22},{7,23},{8,24},{9,... | collective-permute-start | bytes 294920 | tf_op jit(solution)/shard_map/ppermute | solution.py:235
  60.9 2.4 %collective-permute-start.30 = (bf16[24,2048]{1,0:T(8,128)(2,1)S(1)}, bf16[24,2048]{1,0:T(8,128)(2,1)S(1)}, u32[]{:S(2)}, u32[]{:S(2)}) collective-permute-start(bf16[24,2048]{1,0:T(8,128)(2,1)S(1)} %get-tuple-element.34), channel_id=1, source_target_pairs={{0,24},{1,25},{2,26},{3,27},{4,28},{5,29},{6,30},{7,31},{8,16},{9,... | collective-permute-start | bytes 294920 | tf_op jit(solution)/shard_map/ppermute | solution.py:235
  63.5 2.0 %collective-permute-done.29.refs_7_ = bf16[24,2048]{1,0:T(8,128)(2,1)S(1)} collective-permute-done((bf16[24,2048]{1,0:T(8,128)(2,1)S(1)}, bf16[24,2048]{1,0:T(8,128)(2,1)S(1)}, u32[]{:S(2)}, u32[]{:S(2)}) %collective-permute-start.29) | collective-permute-done | bytes 98336 | tf_op jit(solution)/shard_map/ppermute | solution.py:235
  65.8 1.6 %collective-permute-done.30.refs_8_ = bf16[24,2048]{1,0:T(8,128)(2,1)S(1)} collective-permute-done((bf16[24,2048]{1,0:T(8,128)(2,1)S(1)}, bf16[24,2048]{1,0:T(8,128)(2,1)S(1)}, u32[]{:S(2)}, u32[]{:S(2)}) %collective-permute-start.30) | collective-permute-done | bytes 98336 | tf_op jit(solution)/shard_map/ppermute | solution.py:235
  67.4 1.1 %norm.1 = f32[384,128]{1,0:T(8,128)} custom-call(bf16[24,2048]{1,0:T(8,128)(2,1)S(1)} %get-tuple-element.20.refs_0_, f32[96,2048]{1,0:T(8,128)S(1)} %convert_add_fusion.base.refs_1_, f32[24,8]{1,0:T(8,128)S(1)} %shares.1.refs_2_, bf16[24,2048]{1,0:T(8,128)(2,1)S(1)} %collective-permute-done.11.refs_3_, bf16[24,2048]{1,0:T(8,128)(2,1)S(1)} %collective-permute-done.17.refs_4_, ...), custom_call_target="tpu_custom_call" | custom-call | tf_op jit(solution)/shard_map/norm/pallas_call | solution.py:186
  68.5 3.6 %all-to-all-start = ((f32[32,1,1536]{2,1,0:T(1,128)}), f32[32,1,1536]{2,1,0:T(1,128)S(1)}, u32[]{:S(2)}, u32[]{:S(2)}) async-start(f32[32,1,1536]{2,1,0:T(1,128)} %bitcast.7), calls=%async_computation | async-start | bytes 393216 | tf_op jit(solution)/shard_map/all_to_all | solution.py:283
  72.3 8.9 %all-to-all-done = f32[32,1,1536]{2,1,0:T(1,128)S(1)} async-done(((f32[32,1,1536]{2,1,0:T(1,128)}), f32[32,1,1536]{2,1,0:T(1,128)S(1)}, u32[]{:S(2)}, u32[]{:S(2)}) %all-to-all-start) | async-done | bytes 196640 | tf_op jit(solution)/shard_map/all_to_all | solution.py:283
  81.1 1.1 %finish.1 = bf16[64,768]{1,0:T(8,128)(2,1)} custom-call(f32[384,128]{1,0:T(8,128)S(1)} %bitcast.16, f32[1,128]{1,0:T(1,128)S(1)} %get-tuple-element.39.gain, f32[1,128]{1,0:T(1,128)S(1)} %get-tuple-element.40.bias), custom_call_target="tpu_custom_call" | custom-call | tf_op jit(solution)/shard_map/finish/pallas_call | solution.py:217
  (67 shorter events, 5.7 us)
Async XLA Ops:
  0.0 8.4 %collective-permute-start = (bf16[24,2048]{1,0:T(8,128)(2,1)}, bf16[24,2048]{1,0:T(8,128)(2,1)S(1)}, u32[]{:S(2)}, u32[]{:S(2)}) collective-permute-start(bf16[24,2048]{1,0:T(8,128)(2,1)} %refs_2_.1), channel_id=1, source_target_pairs={{0,8},{1,9},{2,10},{3,11},{4,12},{5,13},{6,14},{7,15},{8,0},{9,1},... | collective-permute-start | bytes 294920 | tf_op jit(solution)/shard_map/ppermute | solution.py:235
  3.1 10.6 %collective-permute-start.1 = (bf16[24,2048]{1,0:T(8,128)(2,1)}, bf16[24,2048]{1,0:T(8,128)(2,1)S(1)}, u32[]{:S(2)}, u32[]{:S(2)}) collective-permute-start(bf16[24,2048]{1,0:T(8,128)(2,1)} %refs_2_.1), channel_id=1, source_target_pairs={{0,16},{1,17},{2,18},{3,19},{4,20},{5,21},{6,22},{7,23},{8,24},{9,... | collective-permute-start | bytes 294920 | tf_op jit(solution)/shard_map/ppermute | solution.py:235
  5.6 8.1 %collective-permute-start.2 = (bf16[24,2048]{1,0:T(8,128)(2,1)}, bf16[24,2048]{1,0:T(8,128)(2,1)S(1)}, u32[]{:S(2)}, u32[]{:S(2)}) collective-permute-start(bf16[24,2048]{1,0:T(8,128)(2,1)} %refs_2_.1), channel_id=1, source_target_pairs={{0,24},{1,25},{2,26},{3,27},{4,28},{5,29},{6,30},{7,31},{8,16},{9,... | collective-permute-start | bytes 294920 | tf_op jit(solution)/shard_map/ppermute | solution.py:235
  8.4 8.9 %collective-permute-start.12 = (bf16[48,2048]{1,0:T(8,128)(2,1)S(1)}, bf16[48,2048]{1,0:T(8,128)(2,1)S(1)}, u32[]{:S(2)}, u32[]{:S(2)}) collective-permute-start(bf16[48,2048]{1,0:T(8,128)(2,1)S(1)} %constant_dynamic-update-slice_fusion.refs_0_), channel_id=1, source_target_pairs={{0,4},{1,5},{2,6},{3,7},{4,0},{5,1},{6,2},{7,3},{8,12},{9,13},{10,... | collective-permute-start | bytes 589832 | tf_op jit(solution)/shard_map/ppermute | solution.py:238
  13.7 5.7 %collective-permute-start.13 = (bf16[48,2048]{1,0:T(8,128)(2,1)S(1)}, bf16[48,2048]{1,0:T(8,128)(2,1)S(1)}, u32[]{:S(2)}, u32[]{:S(2)}) collective-permute-start(bf16[48,2048]{1,0:T(8,128)(2,1)S(1)} %constant_dynamic-update-slice_fusion.2.refs_1_), channel_id=1, source_target_pairs={{0,4},{1,5},{2,6},{3,7},{4,0},{5,1},{6,2},{7,3},{8,12},{9,13},{10,... | collective-permute-start | bytes 589832 | tf_op jit(solution)/shard_map/ppermute | solution.py:238
  15.3 6.6 %collective-permute-start.6 = (bf16[48,2048]{1,0:T(8,128)(2,1)S(1)}, bf16[48,2048]{1,0:T(8,128)(2,1)S(1)}, u32[]{:S(2)}, u32[]{:S(2)}) collective-permute-start(bf16[48,2048]{1,0:T(8,128)(2,1)S(1)} %constant_dynamic-update-slice_fusion.refs_0_), channel_id=1, source_target_pairs={{0,2},{1,3},{2,0},{3,1},{4,6},{5,7},{6,4},{7,5},{8,10},{9,11},{10,... | collective-permute-start | bytes 589832 | tf_op jit(solution)/shard_map/ppermute | solution.py:238
  16.8 7.2 %collective-permute-start.7 = (bf16[48,2048]{1,0:T(8,128)(2,1)S(1)}, bf16[48,2048]{1,0:T(8,128)(2,1)S(1)}, u32[]{:S(2)}, u32[]{:S(2)}) collective-permute-start(bf16[48,2048]{1,0:T(8,128)(2,1)S(1)} %constant_dynamic-update-slice_fusion.2.refs_1_), channel_id=1, source_target_pairs={{0,2},{1,3},{2,0},{3,1},{4,6},{5,7},{6,4},{7,5},{8,10},{9,11},{10,... | collective-permute-start | bytes 589832 | tf_op jit(solution)/shard_map/ppermute | solution.py:238
  17.4 7.2 %collective-permute-start.3 = (bf16[48,2048]{1,0:T(8,128)(2,1)S(1)}, bf16[48,2048]{1,0:T(8,128)(2,1)S(1)}, u32[]{:S(2)}, u32[]{:S(2)}) collective-permute-start(bf16[48,2048]{1,0:T(8,128)(2,1)S(1)} %constant_dynamic-update-slice_fusion.refs_0_), channel_id=1, source_target_pairs={{0,1},{1,0},{2,3},{3,2},{4,5},{5,4},{6,7},{7,6},{8,9},{9,8},{10,11... | collective-permute-start | bytes 589832 | tf_op jit(solution)/shard_map/ppermute | solution.py:238
  17.4 12.2 %collective-permute-start.14 = (bf16[48,2048]{1,0:T(8,128)(2,1)S(1)}, bf16[48,2048]{1,0:T(8,128)(2,1)S(1)}, u32[]{:S(2)}, u32[]{:S(2)}) collective-permute-start(bf16[48,2048]{1,0:T(8,128)(2,1)S(1)} %collective-permute-done.12.refs_0_), channel_id=1, source_target_pairs={{0,1},{1,0},{2,3},{3,2},{4,5},{5,4},{6,7},{7,6},{8,9},{9,8},{10,11... | collective-permute-start | bytes 589832 | tf_op jit(solution)/shard_map/ppermute | solution.py:238
  19.5 10.2 %collective-permute-start.15 = (bf16[48,2048]{1,0:T(8,128)(2,1)S(1)}, bf16[48,2048]{1,0:T(8,128)(2,1)S(1)}, u32[]{:S(2)}, u32[]{:S(2)}) collective-permute-start(bf16[48,2048]{1,0:T(8,128)(2,1)S(1)} %collective-permute-done.13.refs_1_), channel_id=1, source_target_pairs={{0,1},{1,0},{2,3},{3,2},{4,5},{5,4},{6,7},{7,6},{8,9},{9,8},{10,11... | collective-permute-start | bytes 589832 | tf_op jit(solution)/shard_map/ppermute | solution.py:238
  21.9 10.2 %collective-permute-start.4 = (bf16[48,2048]{1,0:T(8,128)(2,1)S(1)}, bf16[48,2048]{1,0:T(8,128)(2,1)S(1)}, u32[]{:S(2)}, u32[]{:S(2)}) collective-permute-start(bf16[48,2048]{1,0:T(8,128)(2,1)S(1)} %constant_dynamic-update-slice_fusion.2.refs_1_), channel_id=1, source_target_pairs={{0,1},{1,0},{2,3},{3,2},{4,5},{5,4},{6,7},{7,6},{8,9},{9,8},{10,11... | collective-permute-start | bytes 589832 | tf_op jit(solution)/shard_map/ppermute | solution.py:238
  24.1 8.3 %collective-permute-start.18 = (bf16[48,2048]{1,0:T(8,128)(2,1)S(1)}, bf16[48,2048]{1,0:T(8,128)(2,1)S(1)}, u32[]{:S(2)}, u32[]{:S(2)}) collective-permute-start(bf16[48,2048]{1,0:T(8,128)(2,1)S(1)} %collective-permute-done.6.refs_0_), channel_id=1, source_target_pairs={{0,4},{1,5},{2,6},{3,7},{4,0},{5,1},{6,2},{7,3},{8,12},{9,13},{10,... | collective-permute-start | bytes 589832 | tf_op jit(solution)/shard_map/ppermute | solution.py:238
  24.6 8.2 %collective-permute-start.19 = (bf16[48,2048]{1,0:T(8,128)(2,1)S(1)}, bf16[48,2048]{1,0:T(8,128)(2,1)S(1)}, u32[]{:S(2)}, u32[]{:S(2)}) collective-permute-start(bf16[48,2048]{1,0:T(8,128)(2,1)S(1)} %collective-permute-done.13.refs_1_), channel_id=1, source_target_pairs={{0,2},{1,3},{2,0},{3,1},{4,6},{5,7},{6,4},{7,5},{8,10},{9,11},{10,... | collective-permute-start | bytes 589832 | tf_op jit(solution)/shard_map/ppermute | solution.py:238
  29.6 5.3 %collective-permute-start.8 = (bf16[48,2048]{1,0:T(8,128)(2,1)S(1)}, bf16[48,2048]{1,0:T(8,128)(2,1)S(1)}, u32[]{:S(2)}, u32[]{:S(2)}) collective-permute-start(bf16[48,2048]{1,0:T(8,128)(2,1)S(1)} %collective-permute-done.6.refs_0_), channel_id=1, source_target_pairs={{0,1},{1,0},{2,3},{3,2},{4,5},{5,4},{6,7},{7,6},{8,9},{9,8},{10,11... | collective-permute-start | bytes 589832 | tf_op jit(solution)/shard_map/ppermute | solution.py:238
  29.7 5.7 %collective-permute-start.9 = (bf16[48,2048]{1,0:T(8,128)(2,1)S(1)}, bf16[48,2048]{1,0:T(8,128)(2,1)S(1)}, u32[]{:S(2)}, u32[]{:S(2)}) collective-permute-start(bf16[48,2048]{1,0:T(8,128)(2,1)S(1)} %collective-permute-done.7.refs_1_), channel_id=1, source_target_pairs={{0,1},{1,0},{2,3},{3,2},{4,5},{5,4},{6,7},{7,6},{8,9},{9,8},{10,11... | collective-permute-start | bytes 589832 | tf_op jit(solution)/shard_map/ppermute | solution.py:238
  32.2 7.9 %collective-permute-start.16 = (bf16[96,2048]{1,0:T(8,128)(2,1)S(1)}, bf16[96,2048]{1,0:T(8,128)(2,1)S(1)}, u32[]{:S(2)}, u32[]{:S(2)}) collective-permute-start(bf16[96,2048]{1,0:T(8,128)(2,1)S(1)} %get-tuple-element.30), channel_id=1, source_target_pairs={{0,1},{1,0},{2,3},{3,2},{4,5},{5,4},{6,7},{7,6},{8,9},{9,8},{10,11... | collective-permute-start | bytes 1179656 | tf_op jit(solution)/shard_map/ppermute | solution.py:238
  32.3 5.2 %collective-permute-start.20 = (bf16[48,2048]{1,0:T(8,128)(2,1)S(1)}, bf16[48,2048]{1,0:T(8,128)(2,1)S(1)}, u32[]{:S(2)}, u32[]{:S(2)}) collective-permute-start(bf16[48,2048]{1,0:T(8,128)(2,1)S(1)} %collective-permute-done.18.refs_0_), channel_id=1, source_target_pairs={{0,1},{1,0},{2,3},{3,2},{4,5},{5,4},{6,7},{7,6},{8,9},{9,8},{10,11... | collective-permute-start | bytes 589832 | tf_op jit(solution)/shard_map/ppermute | solution.py:238
  32.8 4.8 %collective-permute-start.21 = (bf16[48,2048]{1,0:T(8,128)(2,1)S(1)}, bf16[48,2048]{1,0:T(8,128)(2,1)S(1)}, u32[]{:S(2)}, u32[]{:S(2)}) collective-permute-start(bf16[48,2048]{1,0:T(8,128)(2,1)S(1)} %collective-permute-done.19.refs_1_), channel_id=1, source_target_pairs={{0,1},{1,0},{2,3},{3,2},{4,5},{5,4},{6,7},{7,6},{8,9},{9,8},{10,11... | collective-permute-start | bytes 589832 | tf_op jit(solution)/shard_map/ppermute | solution.py:238
  34.9 10.8 %collective-permute-start.5 = (bf16[96,2048]{1,0:T(8,128)(2,1)S(1)}, bf16[96,2048]{1,0:T(8,128)(2,1)S(1)}, u32[]{:S(2)}, u32[]{:S(2)}) collective-permute-start(bf16[96,2048]{1,0:T(8,128)(2,1)S(1)} %get-tuple-element.26), channel_id=1, source_target_pairs={{0,1},{1,0},{2,3},{3,2},{4,5},{5,4},{6,7},{7,6},{8,9},{9,8},{10,11... | collective-permute-start | bytes 1179656 | tf_op jit(solution)/shard_map/ppermute | solution.py:238
  37.4 4.4 %collective-permute-start.10 = (bf16[96,2048]{1,0:T(8,128)(2,1)S(1)}, bf16[96,2048]{1,0:T(8,128)(2,1)S(1)}, u32[]{:S(2)}, u32[]{:S(2)}) collective-permute-start(bf16[96,2048]{1,0:T(8,128)(2,1)S(1)} %get-tuple-element.28), channel_id=1, source_target_pairs={{0,1},{1,0},{2,3},{3,2},{4,5},{5,4},{6,7},{7,6},{8,9},{9,8},{10,11... | collective-permute-start | bytes 1179656 | tf_op jit(solution)/shard_map/ppermute | solution.py:238
  39.5 3.4 %collective-permute-start.22 = (bf16[96,2048]{1,0:T(8,128)(2,1)S(1)}, bf16[96,2048]{1,0:T(8,128)(2,1)S(1)}, u32[]{:S(2)}, u32[]{:S(2)}) collective-permute-start(bf16[96,2048]{1,0:T(8,128)(2,1)S(1)} %get-tuple-element.32), channel_id=1, source_target_pairs={{0,1},{1,0},{2,3},{3,2},{4,5},{5,4},{6,7},{7,6},{8,9},{9,8},{10,11... | collective-permute-start | bytes 1179656 | tf_op jit(solution)/shard_map/ppermute | solution.py:238
  40.2 14.3 %collective-permute-start.25 = (bf16[72,2048]{1,0:T(8,128)(2,1)S(1)}, bf16[72,2048]{1,0:T(8,128)(2,1)S(1)}, u32[]{:S(2)}, u32[]{:S(2)}) collective-permute-start(bf16[72,2048]{1,0:T(8,128)(2,1)S(1)} %slice.36), channel_id=1, source_target_pairs={{0,4},{1,5},{2,6},{3,7},{4,0},{5,1},{6,2},{7,3},{8,12},{9,13},{10,... | collective-permute-start | bytes 884744 | tf_op jit(solution)/shard_map/ppermute | solution.py:238
  41.9 15.1 %collective-permute-start.24 = (bf16[72,2048]{1,0:T(8,128)(2,1)S(1)}, bf16[72,2048]{1,0:T(8,128)(2,1)S(1)}, u32[]{:S(2)}, u32[]{:S(2)}) collective-permute-start(bf16[72,2048]{1,0:T(8,128)(2,1)S(1)} %slice.35), channel_id=1, source_target_pairs={{0,2},{1,3},{2,0},{3,1},{4,6},{5,7},{6,4},{7,5},{8,10},{9,11},{10,... | collective-permute-start | bytes 884744 | tf_op jit(solution)/shard_map/ppermute | solution.py:238
  42.5 18.4 %collective-permute-start.17 = (bf16[24,2048]{1,0:T(8,128)(2,1)S(1)}, bf16[24,2048]{1,0:T(8,128)(2,1)S(1)}, u32[]{:S(2)}, u32[]{:S(2)}) collective-permute-start(bf16[24,2048]{1,0:T(8,128)(2,1)S(1)} %slice.33), channel_id=1, source_target_pairs={{0,4},{1,5},{2,6},{3,7},{4,0},{5,1},{6,2},{7,3},{8,12},{9,13},{10,... | collective-permute-start | bytes 294920 | tf_op jit(solution)/shard_map/ppermute | solution.py:238
  43.1 10.8 %collective-permute-start.28 = (bf16[24,2048]{1,0:T(8,128)(2,1)S(1)}, bf16[24,2048]{1,0:T(8,128)(2,1)S(1)}, u32[]{:S(2)}, u32[]{:S(2)}) collective-permute-start(bf16[24,2048]{1,0:T(8,128)(2,1)S(1)} %get-tuple-element.35), channel_id=1, source_target_pairs={{0,6},{1,7},{2,4},{3,5},{4,2},{5,3},{6,0},{7,1},{8,14},{9,15},{10,... | collective-permute-start | bytes 294920 | tf_op jit(solution)/shard_map/ppermute | solution.py:238
  45.7 15.0 %collective-permute-start.26 = (bf16[48,2048]{1,0:T(8,128)(2,1)S(1)}, bf16[48,2048]{1,0:T(8,128)(2,1)S(1)}, u32[]{:S(2)}, u32[]{:S(2)}) collective-permute-start(bf16[48,2048]{1,0:T(8,128)(2,1)S(1)} %pad_maximum_fusion), channel_id=1, source_target_pairs={{0,6},{1,7},{2,4},{3,5},{4,2},{5,3},{6,0},{7,1},{8,14},{9,15},{10,... | collective-permute-start | bytes 589832 | tf_op jit(solution)/shard_map/ppermute | solution.py:238
  54.0 9.5 %collective-permute-start.11 = (bf16[24,2048]{1,0:T(8,128)(2,1)S(1)}, bf16[24,2048]{1,0:T(8,128)(2,1)S(1)}, u32[]{:S(2)}, u32[]{:S(2)}) collective-permute-start(bf16[24,2048]{1,0:T(8,128)(2,1)S(1)} %slice.32), channel_id=1, source_target_pairs={{0,2},{1,3},{2,0},{3,1},{4,6},{5,7},{6,4},{7,5},{8,10},{9,11},{10,... | collective-permute-start | bytes 294920 | tf_op jit(solution)/shard_map/ppermute | solution.py:238
  54.5 8.9 %collective-permute-start.23 = (bf16[24,2048]{1,0:T(8,128)(2,1)S(1)}, bf16[24,2048]{1,0:T(8,128)(2,1)S(1)}, u32[]{:S(2)}, u32[]{:S(2)}) collective-permute-start(bf16[24,2048]{1,0:T(8,128)(2,1)S(1)} %get-tuple-element.38), channel_id=1, source_target_pairs={{0,6},{1,7},{2,4},{3,5},{4,2},{5,3},{6,0},{7,1},{8,14},{9,15},{10,... | collective-permute-start | bytes 294920 | tf_op jit(solution)/shard_map/ppermute | solution.py:238
  57.0 8.5 %collective-permute-start.29 = (bf16[24,2048]{1,0:T(8,128)(2,1)S(1)}, bf16[24,2048]{1,0:T(8,128)(2,1)S(1)}, u32[]{:S(2)}, u32[]{:S(2)}) collective-permute-start(bf16[24,2048]{1,0:T(8,128)(2,1)S(1)} %close.3), channel_id=1, source_target_pairs={{0,16},{1,17},{2,18},{3,19},{4,20},{5,21},{6,22},{7,23},{8,24},{9,... | collective-permute-start | bytes 294920 | tf_op jit(solution)/shard_map/ppermute | solution.py:235
  60.8 5.0 %collective-permute-start.27 = (bf16[24,2048]{1,0:T(8,128)(2,1)S(1)}, bf16[24,2048]{1,0:T(8,128)(2,1)S(1)}, u32[]{:S(2)}, u32[]{:S(2)}) collective-permute-start(bf16[24,2048]{1,0:T(8,128)(2,1)S(1)} %get-tuple-element.33), channel_id=1, source_target_pairs={{0,8},{1,9},{2,10},{3,11},{4,12},{5,13},{6,14},{7,15},{8,0},{9,1},... | collective-permute-start | bytes 294920 | tf_op jit(solution)/shard_map/ppermute | solution.py:235
  60.9 6.5 %collective-permute-start.30 = (bf16[24,2048]{1,0:T(8,128)(2,1)S(1)}, bf16[24,2048]{1,0:T(8,128)(2,1)S(1)}, u32[]{:S(2)}, u32[]{:S(2)}) collective-permute-start(bf16[24,2048]{1,0:T(8,128)(2,1)S(1)} %get-tuple-element.34), channel_id=1, source_target_pairs={{0,24},{1,25},{2,26},{3,27},{4,28},{5,29},{6,30},{7,31},{8,16},{9,... | collective-permute-start | bytes 294920 | tf_op jit(solution)/shard_map/ppermute | solution.py:235
  68.5 12.6 %all-to-all-start = ((f32[32,1,1536]{2,1,0:T(1,128)}), f32[32,1,1536]{2,1,0:T(1,128)S(1)}, u32[]{:S(2)}, u32[]{:S(2)}) async-start(f32[32,1,1536]{2,1,0:T(1,128)} %bitcast.7), calls=%async_computation | async-start | bytes 393216 | tf_op jit(solution)/shard_map/all_to_all | solution.py:283
  (4 other events, 92.2 us)
